TPU v7x, 256 devices: a 4x2x16 block of a 4x16x16 slice. The times are simulated.
256 devices in a mesh: grp: 2 (over y), fs: 16 (over z), tp: 8 (over x, core).
Axes of the slice: x: 4, y: 2, z: 16, core: 2. Of those that a mesh axis runs over, the one named last changes fastest.
The devices are a block of a 4x16x16 slice.
Arguments:
- tokens: bfloat16 [32768, 2048], P(('grp', 'fs', 'tp')), parts along dimension 0, may hold values from -6 to 6
- norm_gains: float32 [4, 2048], replicated, may hold values from 0.1 to 1.9
- query_weight: bfloat16 [2048, 2048], P('fs', 'tp'), may hold values from -0.125 to 0.125
- key_weight: bfloat16 [2048, 2048], P('fs', 'tp'), may hold values from -0.125 to 0.125
- value_weight: bfloat16 [2048, 4096], P('fs', 'tp'), may hold values from -0.125 to 0.125
- swish_weight: bfloat16 [2048, 4096], P('fs', 'tp'), may hold values from -0.125 to 0.125
- mixer_output: bfloat16 [4096, 2048], P('tp', 'fs'), may hold values from -0.09375 to 0.09375
- gate_weight: bfloat16 [2048, 3072], P('fs', 'tp'), may hold values from -0.125 to 0.125
- up_weight: bfloat16 [2048, 3072], P('fs', 'tp'), may hold values from -0.125 to 0.125
- down_weight: bfloat16 [3072, 2048], P('tp', 'fs'), may hold values from -0.109375 to 0.109375
Outputs:
- layer_output: bfloat16 [32768, 2048], P(('grp', 'fs', 'tp')), parts along dimension 0
There are 2 independent parts, one for each index of `grp`. A program takes and returns all parts, laid end to end along the dimension named above; an argument that names none is the same for every part. Nothing has to cross between parts.
All inputs are finite; a program needn't handle non-finite values.
Results may differ from a plain program's by a relative error of at most 0.02.
Values may be sent and summed in bfloat16 or wider, within the bound.
A program may use at most 64 MiB of HBM per device.

v0:
```python
import jax
import jax.numpy as jnp
from jax import lax
from jax.sharding import PartitionSpec as P

H = 8
QK = 256
BLOCK = 128


norm_epsilon = 1e-06
group_epsilon = 0.01


def laid_out(pieces, dim):
    lengths = list(pieces.shape[1:])
    lengths[dim] *= pieces.shape[0]
    return jnp.moveaxis(pieces, 0, dim).reshape(lengths)


def from_everyone(array, axis):
    copies = jnp.broadcast_to(array, (lax.axis_size(axis), *array.shape))
    return lax.all_to_all(copies, axis, split_axis=0, concat_axis=0, tiled=True)


def gather_directly(array, axis, dim):
    return laid_out(from_everyone(array, axis), dim)


def split_up(array, dim, count):
    before, after = (array.shape[:dim], array.shape[dim + 1 :])
    return jnp.moveaxis(array.reshape(*before, count, -1, *after), dim, 0)


def summed_on_arrival(array, axis, dim):
    count = lax.axis_size(axis)
    pieces = lax.all_to_all(split_up(array, dim, count), axis, 0, 0, tiled=True)
    return jnp.sum(pieces.astype(jnp.float32), axis=0)


def sent_together(arrays, axis, dim, along):
    ends, at = ([], 0)
    for a in arrays[:-1]:
        at += a.shape[along]
        ends.append(at)
    both = jnp.concatenate(arrays, axis=along)
    return tuple(jnp.split(lax.all_gather(both, axis, axis=dim, tiled=True), ends, axis=along))


def rms_scale(matrix, gain):
    return (
        matrix * lax.rsqrt(jnp.mean(matrix * matrix, axis=-1, keepdims=True) + norm_epsilon) * gain
    )


def gather_rows(normed):
    return lax.all_gather(normed, "tp", axis=0, tiled=True)


def add_piece(normed, shard_piece):
    return jnp.dot(normed, shard_piece, preferred_element_type=jnp.float32)


def project_out(active, weight_shard):
    whole_weight = gather_directly(weight_shard, "fs", 1)
    return summed_on_arrival(
        jnp.dot(active, whole_weight, preferred_element_type=jnp.float32).astype(jnp.bfloat16),
        "tp",
        0,
    )


def rotate_halves(head_tensors, cosine_table, sine_table):
    half_width = head_tensors.shape[-1] // 2
    lower_half = head_tensors[..., :half_width]
    upper_half = head_tensors[..., half_width:]
    return jnp.concatenate(
        [
            lower_half * cosine_table - upper_half * sine_table,
            lower_half * sine_table + upper_half * cosine_table,
        ],
        axis=-1,
    )


def retention(queries, key_rows, value_rows, log_decay):
    length, head_count, key_width = queries.shape
    value_width = value_rows.shape[-1]
    blocks = length // BLOCK
    query_blocks = queries.reshape(blocks, BLOCK, head_count, key_width)
    key_blocks = key_rows.reshape(blocks, BLOCK, head_count, key_width)
    value_blocks = value_rows.reshape(blocks, BLOCK, head_count, value_width)
    offsets = jnp.arange(BLOCK, dtype=jnp.float32)
    distance = offsets[:, None] - offsets[None, :]
    within = jnp.where(
        distance >= 0, jnp.exp(log_decay[:, None, None] * jnp.maximum(distance, 0.0)), 0.0
    )
    retention_scores = jnp.einsum(
        "cnhd,cmhd->chnm", query_blocks, key_blocks, preferred_element_type=jnp.float32
    )
    local_part = jnp.einsum(
        "chnm,cmhe->cnhe", retention_scores * within[None], value_blocks.astype(jnp.float32)
    )
    key_decay = jnp.exp((BLOCK - 1.0 - offsets)[:, None] * log_decay[None, :])
    query_decay = jnp.exp((offsets + 1.0)[:, None] * log_decay[None, :])
    block_decay = jnp.exp(BLOCK * log_decay)

    def advance(carry_state, inputs):
        query_block, key_block, value_tile = inputs
        carried = (
            jnp.einsum("nhd,hde->nhe", query_block.astype(jnp.float32), carry_state)
            * query_decay[:, :, None]
        )
        decay_weighted = key_block.astype(jnp.float32) * key_decay[:, :, None]
        carry_state = carry_state * block_decay[:, None, None] + jnp.einsum(
            "yui,yua->uia", decay_weighted, value_tile.astype(jnp.float32)
        )
        return (carry_state, carried)

    starting_state = jnp.zeros((head_count, key_width, value_width), jnp.float32)
    _, carried = lax.scan(advance, starting_state, (query_blocks, key_blocks, value_blocks))
    return (local_part + carried).reshape(length, head_count, value_width)


def per_device(
    tokens,
    norm_gains,
    query_weight,
    key_weight,
    value_weight,
    swish_weight,
    mixer_output,
    gate_weight,
    up_weight,
    down_weight,
):
    residual = tokens.astype(jnp.float32)
    normed = gather_rows(rms_scale(residual, norm_gains[0]).astype(jnp.bfloat16))
    gate_whole, up_whole = sent_together((gate_weight, up_weight), "fs", 0, 1)
    pieces = sent_together((query_weight, key_weight, value_weight, swish_weight), "fs", 0, 1)
    raw_query, raw_keys, raw_values, raw_swish = tuple(
        (add_piece(normed, shard_piece) for shard_piece in pieces)
    )
    length = normed.shape[0]
    head_count = raw_query.shape[1] // QK
    positions = jnp.arange(length, dtype=jnp.float32)
    frequency = 10000.0 ** (-jnp.linspace(0.0, 1.0, QK // 2, dtype=jnp.float32))
    angles = positions[:, None] * frequency[None, :]
    cosine_table = jnp.cos(angles)[:, None, :]
    sine_table = jnp.sin(angles)[:, None, :]
    queries = rotate_halves(
        raw_query.reshape(length, head_count, QK), cosine_table, sine_table
    ).astype(jnp.bfloat16)
    key_rows = (
        rotate_halves(raw_keys.reshape(length, head_count, QK), cosine_table, sine_table)
        * QK ** (-0.5)
    ).astype(jnp.bfloat16)
    value_rows = raw_values.reshape(length, head_count, -1).astype(jnp.bfloat16)
    head_index = (lax.axis_index("tp") * head_count + jnp.arange(head_count)).astype(jnp.float32)
    log_decay = -(4.0 / BLOCK) * (BLOCK / (32.0 * length)) ** (head_index / (H - 1))
    retained = retention(queries, key_rows, value_rows, log_decay)
    centred = retained - jnp.mean(retained, axis=-1, keepdims=True)
    normalized = centred * lax.rsqrt(
        jnp.mean(centred * centred, axis=-1, keepdims=True) + group_epsilon
    )
    gated_rows = (jax.nn.silu(raw_swish) * normalized.reshape(length, -1)).astype(jnp.bfloat16)
    mixer_total = project_out(gated_rows, mixer_output)
    after_mixer = residual + rms_scale(mixer_total, norm_gains[1])
    widened = gather_rows(rms_scale(after_mixer, norm_gains[2]).astype(jnp.bfloat16))
    gate_sum = jnp.dot(widened, gate_whole, preferred_element_type=jnp.float32)
    up_sum = jnp.dot(widened, up_whole, preferred_element_type=jnp.float32)
    hidden = (jax.nn.silu(gate_sum) * up_sum).astype(jnp.bfloat16)
    channel = project_out(hidden, down_weight)
    return (after_mixer + rms_scale(channel, norm_gains[3])).astype(jnp.bfloat16)


def solution(mesh):
    placed = (
        P(("grp", "fs", "tp"), None),
        P(),
        P("fs", "tp"),
        P("fs", "tp"),
        P("fs", "tp"),
        P("fs", "tp"),
        P("tp", "fs"),
        P("fs", "tp"),
        P("fs", "tp"),
        P("tp", "fs"),
    )
    return jax.shard_map(
        per_device,
        mesh=mesh,
        in_specs=placed,
        out_specs=P(("grp", "fs", "tp"), None),
        check_vma=False,
    )
```

profile of v0, /device:TPU:33, one launch (start us, length us, event | category | flops | bytes accessed | tf_op | source)
XLA Modules:
  0.0 461.9 jit_solution(14256166903097563935)
XLA Ops:
  8.8 2.0 fusion.41
  13.5 24.7 %all-to-all-start = ((bf16[16,512,128]{1,2,0:T(8,128)(2,1)}), bf16[16,512,128]{1,2,0:T(8,128)(2,1)}, u32[]{:S(2)}, u32[]{:S(2)}) async-start(bf16[16,512,128]{1,2,0:T(8,128)(2,1)} %broadcast_in_dim.19), calls=%async_computation | async-start | bytes 4194304 | tf_op jit(solution)/shard_map/all_to_all | solution.py:23
  39.4 24.8 %all-gather.5.cloned.1.call-done = bf16[1024,2048]{1,0:T(8,128)(2,1)} async-done(((bf16[128,2048]{1,0:T(8,128)(2,1)}), bf16[1024,2048]{1,0:T(8,128)(2,1)}) %all-gather.5.cloned.1.call-update) | async-done | bytes 4194320 | tf_op jit(solution)/shard_map/all_gather | solution.py:57
  64.2 130.5 %all-gather.7.cloned.1.call-done = bf16[2048,1536]{1,0:T(8,128)(2,1)} async-done(((bf16[128,1536]{1,0:T(8,128)(2,1)}), bf16[2048,1536]{1,0:T(8,128)(2,1)}) %all-gather.7.cloned.1.call-update) | async-done | bytes 6291472 | tf_op jit(solution)/shard_map/all_gather | solution.py:47
  194.7 3.9 convolution_bitcast_fusion.2
  199.1 3.4 convolution_bitcast_fusion.3
  202.5 2.3 subtract_convert_fusion
  206.8 3.3 fusion.36
  210.1 25.3 %while.15 = (s32[]{:T(128)}, f32[1,256,512]{2,1,0:T(8,128)S(1)}, f32[8,128,1,512]{3,1,2,0:T(8,128)}, f32[1]{0:T(128)}, bf16[8,128,1,256]{3,2,1,0:T(2,128)(2,1)S(...) while((s32[]{:T(128)}, f32[1,256,512]{2,1,0:T(8,128)S(1)}, ...), condition=%wide.region_2.3_spmd.clone.clone.clone, body=%wide.region_1.2_spmd.clone.clone.clone.sunk | while | flops 67797504 | bytes 2232440 | solution.py:121
  213.3 1.8 fusion.99
  219.7 1.7 fusion.99
  226.0 1.7 fusion.99
  229.2 1.8 fusion.99
  232.3 1.7 fusion.99
  235.5 2.7 fusion.73
  238.6 5.6 %fusion.27 = bf16[1024,512]{1,0:T(8,128)(2,1)S(1)} fusion(f32[8,128,1,512]{3,1,0,2:T(8,128)S(1)} %get-tuple-element.179, bf16[1024,2048]{1,0:T(8,128)(2,1)} %all-gather.5.cloned.1.call-done, bf16[2048,1536]{1,0:T(8,128)(2,1)} %all-gather.7.cloned.1.call-done, f32[1024]{0:T(1024)S(1)} %rsqrt_bitcast_fusion, f32[1024]{0:T(1024)S(1)} %get-tuple-element.174), kind=kOutput, calls=%fused_computation.36 | convolution fusion | flops 2151677952 | bytes 9445376 | tf_op jit(solution)/shard_map/dot_general | solution.py:61
  244.2 4.0 convolution_convert_fusion.1
  248.2 56.0 %all_to_all.20 = bf16[8,128,2048]{2,1,0:T(8,128)(2,1)S(1)} all-to-all(bf16[8,128,2048]{2,1,0:T(8,128)(2,1)S(1)} %bitcast.130), channel_id=1, replica_groups=mesh['grp'=2,'fs'=16,'tp'=8] {'tp'}, dimensions={0} | all-to-all | bytes 8388608 | tf_op jit(solution)/shard_map/all_to_all | solution.py:37
  308.3 8.1 %all-to-all-start.2 = ((bf16[16,384,128]{1,2,0:T(8,128)(2,1)}), bf16[16,384,128]{1,2,0:T(8,128)(2,1)S(1)}, u32[]{:S(2)}, u32[]{:S(2)}) async-start(bf16[16,384,128]{1,2,0:T(8,128)(2,1)} %broadcast_in_dim.20), calls=%async_computation.2 | async-start | bytes 3145728 | tf_op jit(solution)/shard_map/all_to_all | solution.py:23
  316.4 25.5 %all-gather.9.cloned.1.call-done = bf16[1024,2048]{1,0:T(8,128)(2,1)} async-done(((bf16[128,2048]{1,0:T(8,128)(2,1)}), bf16[1024,2048]{1,0:T(8,128)(2,1)}) %all-gather.9.cloned.1.call-update) | async-done | bytes 4194320 | tf_op jit(solution)/shard_map/all_gather | solution.py:57
  342.0 6.2 %fusion.30 = f32[1024,384]{1,0:T(8,128)} fusion(bf16[1024,2048]{1,0:T(8,128)(2,1)} %all-gather.9.cloned.1.call-done, bf16[2048,768]{1,0:T(8,128)(2,1)} %all-gather.11.cloned.1.call-done), kind=kOutput, calls=%fused_computation.40 | convolution fusion | flops 1610612736 | bytes 7340032 | tf_op jit(solution)/shard_map/dot_general | solution.py:170
  348.1 37.1 %all-to-all-done.2 = bf16[16,384,128]{1,2,0:T(8,128)(2,1)S(1)} async-done(((bf16[16,384,128]{1,2,0:T(8,128)(2,1)}), bf16[16,384,128]{1,2,0:T(8,128)(2,1)S(1)}, u32[]{:S(2)}, u32[]{:S(2)}) %all-to-all-start.2) | async-done | bytes 1572896 | tf_op jit(solution)/shard_map/all_to_all | solution.py:23
  385.3 9.6 %convolution_convert_fusion = bf16[1024,2048]{1,0:T(8,128)(2,1)} fusion(bf16[384,2048]{0,1:T(8,128)(2,1)S(1)} %bitcast.137, f32[1024,384]{1,0:T(8,128)} %fusion.30, bf16[1024,2048]{1,0:T(8,128)(2,1)} %all-gather.9.cloned.1.call-done, bf16[2048,768]{1,0:T(8,128)(2,1)} %all-gather.11.cloned.1.call-done), kind=kOutput, calls=%fused_computation.26 | convolution fusion | flops 3225681920 | bytes 13107200 | tf_op jit(solution)/shard_map/dot_general | solution.py:67
  394.9 58.4 %all_to_all.21 = bf16[8,128,2048]{2,1,0:T(8,128)(2,1)S(1)} all-to-all(bf16[8,128,2048]{2,1,0:T(8,128)(2,1)} %bitcast.129), channel_id=1, replica_groups=mesh['grp'=2,'fs'=16,'tp'=8] {'tp'}, dimensions={0} | all-to-all | bytes 8388608 | tf_op jit(solution)/shard_map/all_to_all | solution.py:37
  (90 shorter events, 31.2 us)
Async XLA Ops:
  6.5 4.4 copy-start.9
  6.5 4.5 copy-start.8
  6.6 4.5 copy-start.4
  6.6 4.5 copy-start.3
  6.6 5.3 %copy-start.2 = (bf16[512,128]{1,0:T(8,128)(2,1)S(1)}, bf16[512,128]{1,0:T(8,128)(2,1)}, u32[]{:S(2)}) copy-start(bf16[512,128]{1,0:T(8,128)(2,1)} %param.18) | copy-start | bytes 393220
  6.6 57.6 %all-gather.5.cloned.1.call-start = ((), (), s32[]{:S(2)}) async-start(), calls=%async_computation.4 | async-start | bytes 4718592 | tf_op jit(solution)/shard_map/all_gather | solution.py:57
  10.9 183.8 %all-gather.7.cloned.1.call-start = ((), (), s32[]{:S(2)}) async-start(), calls=%async_computation.5 | async-start | bytes 6684672 | tf_op jit(solution)/shard_map/all_gather | solution.py:47
  13.5 24.7 %copy-start.6 = (bf16[128,384]{1,0:T(8,128)(2,1)S(1)}, bf16[128,384]{1,0:T(8,128)(2,1)}, u32[]{:S(2)}) copy-start(bf16[128,384]{1,0:T(8,128)(2,1)} %param.20) | copy-start | bytes 294916
  13.5 24.7 %copy-start.7 = (bf16[128,384]{1,0:T(8,128)(2,1)S(1)}, bf16[128,384]{1,0:T(8,128)(2,1)}, u32[]{:S(2)}) copy-start(bf16[128,384]{1,0:T(8,128)(2,1)} %param.19) | copy-start | bytes 294916
  13.5 230.7 %all-to-all-start = ((bf16[16,512,128]{1,2,0:T(8,128)(2,1)}), bf16[16,512,128]{1,2,0:T(8,128)(2,1)}, u32[]{:S(2)}, u32[]{:S(2)}) async-start(bf16[16,512,128]{1,2,0:T(8,128)(2,1)} %broadcast_in_dim.19), calls=%async_computation | async-start | bytes 4194304 | tf_op jit(solution)/shard_map/all_to_all | solution.py:23
  38.2 278.3 %all-gather.11.cloned.1.call-start = ((), (), s32[]{:S(2)}) async-start(), calls=%async_computation.7 | async-start | bytes 3342336 | tf_op jit(solution)/shard_map/all_gather | solution.py:47
  39.0 302.9 %all-gather.9.cloned.1.call-start = ((), (), s32[]{:S(2)}) async-start(), calls=%async_computation.6 | async-start | bytes 4718592 | tf_op jit(solution)/shard_map/all_gather | solution.py:57
  194.7 4.4 copy-start.10
  202.5 4.3 copy-start.11
  204.8 5.3 %copy-start.1 = (bf16[1024,1,128]{2,0,1:T(8,128)(2,1)}, bf16[1024,1,128]{2,0,1:T(8,128)(2,1)S(1)}, u32[]{:S(2)}) copy-start(bf16[1024,1,128]{2,0,1:T(8,128)(2,1)S(1)} %get-tuple-element.167) | copy-start | bytes 786436
  304.2 1.0 copy-start
  305.3 1.5 copy-start.5
  308.3 77.0 %all-to-all-start.2 = ((bf16[16,384,128]{1,2,0:T(8,128)(2,1)}), bf16[16,384,128]{1,2,0:T(8,128)(2,1)S(1)}, u32[]{:S(2)}, u32[]{:S(2)}) async-start(bf16[16,384,128]{1,2,0:T(8,128)(2,1)} %broadcast_in_dim.20), calls=%async_computation.2 | async-start | bytes 3145728 | tf_op jit(solution)/shard_map/all_to_all | solution.py:23
Sparse Core Ops, SparseCore 0:
  11.0 53.0 all-gather.4
  66.0 128.6 all-gather.6
  196.5 65.3 all-gather.10
  306.9 34.9 all-gather.8
where the time goes:
time: 463 us; the launch traced here: 462 us
  waiting for transfers between devices  218 us (47%)
  blocking collectives  114 us (25%)
  matrix products  62 us (13%)
  starting transfers between devices  33 us (7%)
  other arithmetic  15.7 us (3%)
  between operations  13.5 us (3%)
  local copies, waits for them, and re-layouts  4.77 us (1%)
    all_gather x2, waiting for transfers between devices, sent_together(): lax.all_gather(both, axis, axis=dim, tiled=True)  131 us
    all_to_all x2, blocking collectives, summed_on_arrival(): pieces = lax.all_to_all(split_up(array, dim, count), axis, 0, 0, tiled=True)  114 us
    all_gather x2, waiting for transfers between devices, gather_rows(): return lax.all_gather(normed, 'tp', axis=0, tiled=True)  50.3 us
    all_to_all x2, waiting for transfers between devices, from_everyone(): return lax.all_to_all(copies, axis, split_axis=0, concat_axis=0, tiled=True)  37.1 us
    all_to_all x2, starting transfers between devices, from_everyone(): return lax.all_to_all(copies, axis, split_axis=0, concat_axis=0, tiled=True)  32.7 us
    dot_general x4, matrix products, add_piece(): return jnp.dot(normed, shard_piece, preferred_element_type=jnp.float32)  16.2 us
    dot_general x8, matrix products, advance(): jnp.einsum('nhd,hde->nhe', query_block.astype(jnp.float32), carry_state)  14 us
    dot_general x2, matrix products, project_out(): jnp.dot(active, whole_weight, preferred_element_type=jnp.float32)  13.6 us
  transfers between devices with their start and end apart: 6, of which 4 were waited for; matrix products, arithmetic and copies ran while one was open for 14% of the time, Pallas kernels for 0%

commit v1 on v0

v1 whole, which is shorter than its diff:
```python
import functools

import jax
import jax.numpy as jnp
import numpy as np
from jax import lax
from jax.experimental import pallas as pl
from jax.experimental.pallas import tpu as pltpu
from jax.sharding import PartitionSpec as P

H = 8
BLOCK = 128
norm_epsilon = 1e-06
group_epsilon = 0.01
MESH = pl.DeviceIdType.MESH
F32 = jnp.float32
BF16 = jnp.bfloat16


def mod(a, n):
    return lax.rem(a + n, n)


def rms(matrix):
    return matrix * lax.rsqrt(jnp.mean(matrix * matrix, axis=-1, keepdims=True) + norm_epsilon)


def silu(v):
    return v / (1.0 + jnp.exp(-v))


def kernel(
    nf,
    nx,
    tok,
    gains,
    lam_ref,
    cos_hbm,
    sin_hbm,
    wq,
    wk,
    wv,
    ws,
    wo,
    wg,
    wu,
    wd,
    out,
    w1,
    w2,
    w3,
    w4,
    xn,
    xw,
    acc,
    qb,
    kb,
    vb,
    gp,
    hid,
    part,
    sib_in,
    stage,
    pass_in,
    from_left,
    from_right,
    am,
    cos,
    sin,
    decay,
    local_sem,
    z_send,
    z_recv,
    y_send,
    y_recv,
    g_send,
    g_recv,
    s_send,
    s_recv,
    r_send,
    r_recv,
):
    rows, width = tok.shape
    seq = xn.shape[0]
    half = width // 2
    quarter = seq // 4
    me = lax.axis_index("fs")
    tp = lax.axis_index("tp")
    group = lax.axis_index("grp")
    x = tp // 2
    core = lax.rem(tp, 2)
    plane = lax.rem(group, 2)
    up = {"fs": mod(me + 1, nf)}
    down = {"fs": mod(me - 1, nf)}
    pair = {"grp": group + 1 - 2 * plane}
    sib = {"tp": 2 * x + 1 - core}
    right = {"tp": 2 * mod(x + 1, nx) + core}
    left = {"tp": 2 * mod(x - 1, nx) + core}

    def copy(src, dst, send, recv, device):
        return pltpu.make_async_remote_copy(
            src_ref=src,
            dst_ref=dst,
            send_sem=send,
            recv_sem=recv,
            device_id=device,
            device_id_type=MESH,
        )

    kd = wq.shape[0]
    mine = pl.ds(pl.multiple_of(me * kd, kd), kd)
    mine_cols = pl.ds(pl.multiple_of(me * kd, kd), kd)
    qw, vw, ff = wq.shape[1], wv.shape[1], wg.shape[1]
    locals_ = [
        (wq, w1.at[mine, 0:qw]),
        (wk, w1.at[mine, qw : 2 * qw]),
        (wv, w1.at[mine, 2 * qw : 2 * qw + vw]),
        (ws, w1.at[mine, 2 * qw + vw : 2 * qw + 2 * vw]),
        (wo, w2.at[:, mine_cols]),
        (wg, w3.at[mine, 0:ff]),
        (wu, w3.at[mine, ff : 2 * ff]),
        (wd, w4.at[:, mine_cols]),
        (cos_hbm, cos),
        (sin_hbm, sin),
    ]
    loads = [
        pltpu.make_async_copy(src, dst, local_sem.at[i]) for i, (src, dst) in enumerate(locals_)
    ]
    for load in loads:
        load.start()

    barrier = pltpu.get_barrier_semaphore()
    for device in (up, down, pair, sib, right, left):
        pl.semaphore_signal(barrier, inc=1, device_id=device, device_id_type=MESH)

    own = pl.multiple_of(tp * rows, rows)

    def norm_in(i, carry):
        at = pl.multiple_of(i * 16, 16)
        value = rms(tok[pl.ds(at, 16), :].astype(F32)) * gains[0:1, :]
        xn[pl.ds(own + at, 16), :] = value.astype(BF16)
        return carry

    lax.fori_loop(0, rows // 16, norm_in, 0)
    pl.semaphore_wait(barrier, 6)

    def third(total):
        return total // 3 // 16 * 16 + (16 if total // 3 % 16 else 0)

    def place(a, owner, piece, plane_, rows_half=None):
        ref = (w1, w2, w3, w4)[a]
        if a in (0, 2):
            w = ref.shape[1] // 3
            start, count = owner * kd, kd
            if rows_half is not None:
                count = kd // 2
                start = start + rows_half * count
            r = pl.ds(pl.multiple_of(start, kd // 2), count)
            c = pl.ds(pl.multiple_of(plane_ * 2 * w, 128), w) if piece == 0 else pl.ds(w, w)
            return ref.at[r, c]
        t = third(ref.shape[0])
        mid = ref.shape[0] - 2 * t
        r = pl.ds(pl.multiple_of(plane_ * (t + mid), 16), t) if piece == 0 else pl.ds(t, mid)
        return ref.at[r, pl.ds(pl.multiple_of(owner * kd, kd), kd)]

    def owner_of(d, s):
        return mod(me - s, nf) if d == 0 else lax.rem(me + s, nf)

    far = nf // 2

    def z_copy(a, d, piece, s, rows_half=None):
        src = place(a, owner_of(d, s - 1), piece, plane, rows_half)
        k = (a * 2 + d) * 2 + piece
        return copy(src, src, z_send.at[k], z_recv.at[k, s - 1], up if d == 0 else down)

    def z_arrived(a, d, piece, s, rows_half=None):
        dst = place(a, owner_of(d, s), piece, plane, rows_half)
        k = (a * 2 + d) * 2 + piece
        copy(dst, dst, z_send.at[k], z_recv.at[k, s - 1], up if d == 0 else down).wait_recv()

    def y_copy(a, d, s, rows_half=None):
        src = place(a, owner_of(d, s), 0, plane, rows_half)
        k = a * 2 + d
        return copy(src, src, y_send.at[k], y_recv.at[k, s - 1], pair)

    def y_arrived(a, d, s, rows_half=None):
        dst = place(a, owner_of(d, s), 0, 1 - plane, rows_half)
        k = a * 2 + d
        copy(dst, dst, y_send.at[k], y_recv.at[k, s - 1], pair).wait_recv()

    def last_half(a, d):
        return d if a in (0, 2) else None

    def has_last(a, d):
        return a in (0, 2) or (a == 1 and d == 0) or (a == 3 and d == 1)

    def pump_start(arrays):
        for piece in (0, 1):
            for a in arrays:
                for d in (0, 1):
                    z_copy(a, d, piece, 1).start()

    def pump(arrays, s, first=False):
        for piece in (0, 1):
            for a in arrays:
                for d in (0, 1):
                    z_arrived(a, d, piece, s)
                    z_copy(a, d, piece, s).wait_send()
                    z_copy(a, d, piece, s + 1).start()
                    if piece == 0:
                        if not first:
                            y_copy(a, d, s - 1).wait_send()
                        y_copy(a, d, s).start()

    def pump_before_last(arrays):
        s = far - 1
        for piece in (0, 1):
            for a in arrays:
                for d in (0, 1):
                    z_arrived(a, d, piece, s)
                    z_copy(a, d, piece, s).wait_send()
                    if has_last(a, d):
                        z_copy(a, d, piece, s + 1, last_half(a, d)).start()
                    if piece == 0:
                        y_copy(a, d, s - 1).wait_send()
                        y_copy(a, d, s).start()

    def pump_last(arrays):
        for piece in (0, 1):
            for a in arrays:
                for d in (0, 1):
                    if has_last(a, d):
                        z_arrived(a, d, piece, far, last_half(a, d))
                        z_copy(a, d, piece, far, last_half(a, d)).wait_send()
                    if piece == 0:
                        y_copy(a, d, far - 1).wait_send()
                        if has_last(a, d):
                            y_copy(a, d, far, last_half(a, d)).start()

    def y_all(a, s):
        for d in (0, 1):
            if s is far:
                if has_last(a, d):
                    y_arrived(a, d, far, last_half(a, d))
            else:
                y_arrived(a, d, s)

    def y_drain(a):
        for d in (0, 1):
            if has_last(a, d):
                y_copy(a, d, far, last_half(a, d)).wait_send()

    def gather(n, ref, block):
        at_left, at_right, at_far = mod(x - 1, nx), mod(x + 1, nx), mod(x + 2, nx)
        lo, hi = pl.ds(0, half), pl.ds(half, half)
        every = pl.ds(0, width)

        def whole(xx, cc, cols=every):
            return ref.at[pl.ds(pl.multiple_of(block(xx, cc) * rows, rows), rows), cols]

        def send(k, xx, cols, device):
            src = whole(xx, core, cols)
            return copy(src, src, g_send.at[n, k], g_recv.at[n, k], device)

        def arrived(k, xx, cc, cols):
            dst = whole(xx, cc, cols)
            copy(dst, dst, g_send.at[n, k], g_recv.at[n, k], sib).wait_recv()

        sends = []

        def go(*args):
            s = send(*args)
            s.start()
            sends.append(s)

        def first():
            go(1, x, every, right)
            go(2, x, every, left)
            go(0, x, every, sib)

        def second():
            arrived(1, at_left, core, every)
            go(3, at_left, lo, right)
            go(4, at_left, every, sib)
            arrived(2, at_right, core, every)
            go(5, at_right, hi, left)
            go(6, at_right, every, sib)

        def third_():
            arrived(3, at_far, core, lo)
            go(7, at_far, lo, sib)
            arrived(5, at_far, core, hi)
            go(8, at_far, hi, sib)

        def own_chip():
            arrived(0, x, 1 - core, every)

        def near():
            arrived(4, at_left, 1 - core, every)
            arrived(6, at_right, 1 - core, every)

        def rest():
            arrived(7, at_far, 1 - core, lo)
            arrived(8, at_far, 1 - core, hi)

        def drain():
            for s in sends:
                s.wait_send()

        return first, second, third_, own_chip, near, rest, drain

    for load in loads[:5]:
        load.wait()
    pump_start((0, 1))
    first, second, third_, own_chip, near, rest, drain1 = gather(0, xn, lambda xx, cc: 2 * xx + cc)
    first()

    lam = lam_ref[0:1, 0:1]
    dn = lax.broadcasted_iota(jnp.int32, decay.shape, 0) + (seq - quarter)
    dm = lax.broadcasted_iota(jnp.int32, decay.shape, 1)
    dist = (dn - dm).astype(F32)
    decay[...] = jnp.where(dist >= 0.0, jnp.exp(lam * jnp.maximum(dist, 0.0)), 0.0)
    for load in loads[5:]:
        load.wait()

    def k_slice(owner):
        return pl.ds(pl.multiple_of(owner * kd, kd), kd)

    def add_own():
        def body(i, carry):
            r = pl.ds(pl.multiple_of(i * quarter, quarter), quarter)
            acc[r, :] = jnp.dot(
                xn[r, k_slice(me)], w1[k_slice(me), :], preferred_element_type=F32
            )
            return carry

        lax.fori_loop(0, 4, body, 0)

    def add_two(s):
        a, b = k_slice(owner_of(0, s)), k_slice(owner_of(1, s))

        def body(i, carry):
            r = pl.ds(pl.multiple_of(i * quarter, quarter), quarter)
            acc[r, :] = (
                acc[r, :]
                + jnp.dot(xn[r, a], w1[a, :], preferred_element_type=F32)
                + jnp.dot(xn[r, b], w1[b, :], preferred_element_type=F32)
            )
            return carry

        lax.fori_loop(0, 4, body, 0)

    pump((0, 1), 1, first=True)
    second()
    pump((0, 1), 2)
    own_chip()
    third_()
    near()
    rest()
    add_own()
    y_all(0, 1)
    add_two(1)

    def steps(s, carry):
        pump((0, 1), s)
        y_all(0, s - 1)
        add_two(s - 1)
        return carry

    lax.fori_loop(3, far - 1, steps, 0)
    pump_before_last((0, 1))
    pump_start((2, 3))
    y_all(0, far - 2)
    add_two(far - 2)
    pump_last((0, 1))
    y_all(0, far - 1)
    add_two(far - 1)
    y_all(0, far)
    far_slice = k_slice(owner_of(0, far))

    key_scale = float(qw) ** -0.5
    hq = qw // 2

    def finish(i, carry):
        r = pl.ds(pl.multiple_of(i * quarter, quarter), quarter)
        total = acc[r, :] + jnp.dot(xn[r, far_slice], w1[far_slice, :], preferred_element_type=F32)
        c, s = cos[r, :], sin[r, :]
        for ref, at, scale in ((qb, 0, None), (kb, qw, key_scale)):
            a, b = total[:, at : at + hq], total[:, at + hq : at + qw]
            first_half = a * c - b * s
            second_half = a * s + b * c
            if scale is not None:
                first_half, second_half = first_half * scale, second_half * scale
            ref[r, 0:hq] = first_half.astype(BF16)
            ref[r, hq:qw] = second_half.astype(BF16)
        vb[r, :] = total[:, 2 * qw : 2 * qw + vw].astype(BF16)
        acc[r, 2 * qw + vw :] = total[:, 2 * qw + vw :]
        return carry

    lax.fori_loop(0, 4, finish, 0)
    pump((2, 3), 1, first=True)

    def retain(i):
        r = slice(i * quarter, (i + 1) * quarter)
        seen = (i + 1) * quarter
        scores = lax.dot_general(
            qb[r, :], kb[0:seen, :], (((1,), (1,)), ((), ())), preferred_element_type=F32
        )
        weighted = (scores * decay[:, seq - seen :]).astype(BF16)
        retained = jnp.dot(weighted, vb[0:seen, :], preferred_element_type=F32)
        centred = retained - jnp.mean(retained, axis=-1, keepdims=True)
        normalized = centred * lax.rsqrt(
            jnp.mean(centred * centred, axis=-1, keepdims=True) + group_epsilon
        )
        gated = (silu(acc[r, 2 * qw + vw :]) * normalized).astype(BF16)
        gp[i * rows : (i + 1) * rows, :] = gated[0:rows, :]
        gp[(nx + i) * rows : (nx + i + 1) * rows, :] = gated[rows:, :]

    retain(0)
    retain(1)
    pump((2, 3), 2)
    retain(2)
    retain(3)
    y_all(1, 1)
    for s in range(2, far):
        y_all(1, s)
    y_all(1, far)
    pump((2, 3), 3)

    def project(lhs, weight, cc):
        r = pl.ds(pl.multiple_of(cc * nx * rows, rows), nx * rows)
        n = width // 4

        def body(j, carry):
            cols = pl.ds(pl.multiple_of(j * n, n), n)
            part[r, cols] = jnp.dot(lhs[r, :], weight[:, cols], preferred_element_type=F32).astype(
                BF16
            )
            return carry

        lax.fori_loop(0, 4, body, 0)

    def reduce(n, lhs, weight, pumps):
        lo, hi = slice(0, half), slice(half, width)
        near_x = (mod(x + 2, nx), mod(x + 1, nx), mod(x - 1, nx), x)

        def rows_of(cc, xx):
            return pl.ds(pl.multiple_of((cc * nx + xx) * rows, rows), rows)

        project(lhs, weight, 1 - core)
        sends = []
        arrivals = []
        for k, xx in enumerate(near_x):
            s = copy(
                part.at[rows_of(1 - core, xx), :],
                sib_in.at[n, k],
                s_send.at[n, k],
                s_recv.at[n, k],
                sib,
            )
            s.start()
            sends.append(s)
            arrivals.append(s)
        project(lhs, weight, core)

        def pre(k, cols):
            return part[rows_of(core, near_x[k]), cols].astype(F32) + sib_in[n, k, :, cols].astype(
                F32
            )

        def ship(k, src, dst, device):
            s = copy(src, dst, r_send.at[n, k], r_recv.at[n, k], device)
            s.start()
            sends.append(s)
            arrivals.append(s)

        arrivals[0].wait_recv()
        stage[n, 0, :, hi] = pre(0, hi).astype(BF16)
        ship(0, stage.at[n, 0, :, hi], pass_in.at[n, 0], right)
        stage[n, 0, :, lo] = pre(0, lo).astype(BF16)
        ship(1, stage.at[n, 0, :, lo], pass_in.at[n, 1], left)
        arrivals[1].wait_recv()
        stage[n, 1, :, lo] = pre(1, lo).astype(BF16)
        ship(2, stage.at[n, 1, :, lo], from_left.at[n, :, lo], right)
        arrivals[2].wait_recv()
        stage[n, 2, :, hi] = pre(2, hi).astype(BF16)
        ship(3, stage.at[n, 2, :, hi], from_right.at[n, :, hi], left)
        pumps[0]()
        arrivals[4].wait_recv()
        stage[n, 1, :, hi] = (pre(1, hi) + pass_in[n, 0].astype(F32)).astype(BF16)
        ship(4, stage.at[n, 1, :, hi], from_left.at[n, :, hi], right)
        arrivals[5].wait_recv()
        stage[n, 2, :, lo] = (pre(2, lo) + pass_in[n, 1].astype(F32)).astype(BF16)
        ship(5, stage.at[n, 2, :, lo], from_right.at[n, :, lo], left)
        arrivals[3].wait_recv()
        pumps[1]()
        for k in (6, 7, 8, 9):
            arrivals[k].wait_recv()

        def total(at, count):
            r = pl.ds(at, count)
            here = part[pl.ds((core * nx + x) * rows + at, count), :].astype(F32)
            return (
                (here + sib_in[n, 3, r, :].astype(F32))
                + from_left[n, r, :].astype(F32)
                + from_right[n, r, :].astype(F32)
            )

        def drain():
            for s in sends:
                s.wait_send()

        return total, drain

    def pumps_a():
        pump((2, 3), 4)

    def pumps_b():
        pump((2, 3), 5)
        pump((2, 3), 6)

    total, drain2 = reduce(0, gp, w2, (pumps_a, pumps_b))
    wide_own = (core * nx + x) * rows

    def mixed(i, carry):
        at = pl.multiple_of(i * 16, 16)
        after = tok[pl.ds(at, 16), :].astype(F32) + rms(total(at, 16)) * gains[1:2, :]
        am[pl.ds(at, 16), :] = after
        xw[pl.ds(pl.multiple_of(wide_own + at, 16), 16), :] = (rms(after) * gains[2:3, :]).astype(
            BF16
        )
        return carry

    lax.fori_loop(0, rows // 16, mixed, 0)
    first, second, third_, own_chip, near, rest, drain3 = gather(1, xw, lambda xx, cc: cc * nx + xx)
    first()
    pump_before_last((2, 3))
    second()
    pump_last((2, 3))
    for a in (2, 3):
        for s in range(1, far):
            y_all(a, s)
        y_all(a, far)
    own_chip()
    third_()
    near()
    rest()
    drain2()

    def feed(i, carry):
        r = pl.ds(pl.multiple_of(i * quarter, quarter), quarter)
        both = jnp.dot(xw[r, :], w3[...], preferred_element_type=F32)
        hid[r, :] = (silu(both[:, 0:ff]) * both[:, ff:]).astype(BF16)
        return carry

    lax.fori_loop(0, 4, feed, 0)
    total, drain4 = reduce(1, hid, w4, (lambda: None, lambda: None))

    def last(i, carry):
        at = pl.multiple_of(i * 16, 16)
        r = pl.ds(at, 16)
        out[r, :] = (am[r, :] + rms(total(at, 16)) * gains[3:4, :]).astype(BF16)
        return carry

    lax.fori_loop(0, rows // 16, last, 0)
    drain1()
    drain3()
    drain4()
    for a in range(4):
        y_drain(a)


def layer(nf, nx, tokens, gains, wq, wk, wv, ws, wo, wg, wu, wd):
    rows, width = tokens.shape
    seq = rows * 2 * nx
    qw, vw, ff = wq.shape[1], wv.shape[1], wg.shape[1]
    frequency = 10000.0 ** (-np.linspace(0.0, 1.0, qw // 2))
    angles = np.arange(seq, dtype=np.float64)[:, None] * frequency[None, :]
    cos = jnp.asarray(np.cos(angles).astype(np.float32))
    sin = jnp.asarray(np.sin(angles).astype(np.float32))
    head = lax.axis_index("tp").astype(F32)
    lam = -(4.0 / BLOCK) * (BLOCK / (32.0 * seq)) ** (head / (H - 1))
    lam = jnp.full((8, 128), lam, F32)
    vmem = pl.BlockSpec(memory_space=pltpu.VMEM)
    hbm = pl.BlockSpec(memory_space=pl.ANY)
    dma = pltpu.SemaphoreType.DMA
    far = nf // 2
    half = width // 2
    n1 = 2 * qw + 2 * vw
    return pl.pallas_call(
        functools.partial(kernel, nf, nx),
        out_shape=jax.ShapeDtypeStruct((rows, width), BF16),
        in_specs=[vmem] * 3 + [hbm] * 10,
        out_specs=vmem,
        scratch_shapes=[
            pltpu.VMEM((width, n1), BF16),
            pltpu.VMEM((wo.shape[0], width), BF16),
            pltpu.VMEM((width, 2 * ff), BF16),
            pltpu.VMEM((wd.shape[0], width), BF16),
            pltpu.VMEM((seq, width), BF16),
            pltpu.VMEM((seq, width), BF16),
            pltpu.VMEM((seq, n1), F32),
            pltpu.VMEM((seq, qw), BF16),
            pltpu.VMEM((seq, qw), BF16),
            pltpu.VMEM((seq, vw), BF16),
            pltpu.VMEM((seq, vw), BF16),
            pltpu.VMEM((seq, ff), BF16),
            pltpu.VMEM((seq, width), BF16),
            pltpu.VMEM((2, nx, rows, width), BF16),
            pltpu.VMEM((2, 3, rows, width), BF16),
            pltpu.VMEM((2, 2, rows, half), BF16),
            pltpu.VMEM((2, rows, width), BF16),
            pltpu.VMEM((2, rows, width), BF16),
            pltpu.VMEM((rows, width), F32),
            pltpu.VMEM((seq, qw // 2), F32),
            pltpu.VMEM((seq, qw // 2), F32),
            pltpu.VMEM((seq // 4, seq), F32),
            dma((10,)),
            dma((16,)),
            dma((16, far)),
            dma((8,)),
            dma((8, far)),
            dma((2, 9)),
            dma((2, 9)),
            dma((2, 4)),
            dma((2, 4)),
            dma((2, 6)),
            dma((2, 6)),
        ],
        compiler_params=pltpu.CompilerParams(
            collective_id=0, has_side_effects=True, vmem_limit_bytes=66_000_000
        ),
    )(tokens, gains, lam, cos, sin, wq, wk, wv, ws, wo, wg, wu, wd)


def solution(mesh):
    placed = (
        P(("grp", "fs", "tp"), None),
        P(),
        P("fs", "tp"),
        P("fs", "tp"),
        P("fs", "tp"),
        P("fs", "tp"),
        P("tp", "fs"),
        P("fs", "tp"),
        P("fs", "tp"),
        P("tp", "fs"),
    )
    nf, nt = mesh.shape["fs"], mesh.shape["tp"]
    assert mesh.shape["grp"] % 2 == 0 and nt == 8 and nf % 2 == 0
    return jax.shard_map(
        functools.partial(layer, nf, nt // 2),
        mesh=mesh,
        in_specs=placed,
        out_specs=P(("grp", "fs", "tp"), None),
        check_vma=False,
    )
```

time: 463 us -> 187 us (0.40)
  waiting for transfers between devices: 218 us -> 0 us
  Pallas kernels: 0 us -> 185 us
  blocking collectives: 114 us -> 0 us
  matrix products: 62 us -> 0 us
  starting transfers between devices: 33 us -> 0 us
  other arithmetic: 15.7 us -> 0 us
  between operations: 13.5 us -> 0.06 us
    pallas_call x0 -> x1, Pallas kernels: none -> 185 us  [layer(): pl.pallas_call(functools.partial(kernel, nf, nx), out_shape=jax.ShapeDtyp...]
    all_gather x4 -> x0, waiting for transfers between devices: 181 us -> none  [the longest x2 131 us: sent_together(): lax.all_gather(both, axis, axis=dim, tiled=True)]
    all_to_all x2 -> x0, blocking collectives: 114 us -> none  [summed_on_arrival(): pieces = lax.all_to_all(split_up(array, dim, count), axis, 0, 0, tiled=True)]
    dot_general x24 -> x0, matrix products: 62 us -> none  [the longest x4 16.2 us: add_piece(): return jnp.dot(normed, shard_piece, preferred_element_type=jnp.float32)]
    all_to_all x2 -> x0, waiting for transfers between devices: 37.1 us -> none  [from_everyone(): return lax.all_to_all(copies, axis, split_axis=0, concat_axis=0, tiled=True)]
    all_to_all x2 -> x0, starting transfers between devices: 32.7 us -> none  [from_everyone(): return lax.all_to_all(copies, axis, split_axis=0, concat_axis=0, tiled=True)]
    convert_element_type x4 -> x0, other arithmetic: 5.43 us -> none  [the longest x1 2.03 us: per_device(): rms_scale(residual, norm_gains[0]).astype(jnp.bfloat16)]
  transfers between devices with their start and end apart: 6 -> 0, of which waited for: 4 -> 0; matrix products, arithmetic and copies ran while one was open for 14% -> 0% of each run, Pallas kernels for 0% -> 0%
where the time goes in v1:
time: 187 us
  Pallas kernels  185 us (99%)
  local copies, waits for them, and re-layouts  2.48 us (1%)
    pallas_call x1, Pallas kernels, layer(): pl.pallas_call(functools.partial(kernel, nf, nx), out_shape=jax.ShapeDtyp...  185 us

profile of v1, /device:TPU:33, one launch (start us, length us, event | category | flops | bytes accessed | tf_op | source)
XLA Modules:
  0.0 187.2 jit_solution(17476016666827828700)
XLA Ops:
  0.0 0.6 broadcast_in_dim.3.lam_ref
  0.6 184.7 %shard_map.118 = bf16[128,2048]{1,0:T(8,128)(2,1)} custom-call(bf16[128,2048]{1,0:T(8,128)(2,1)} %tok.1, f32[4,2048]{1,0:T(4,128)} %gains.1, f32[8,128]{1,0:T(8,128)} %broadcast_in_dim.3.lam_ref, f32[1024,128]{1,0:T(8,128)} %constant.15.clone.cos_hbm, f32[1024,128]{1,0:T(8,128)} %constant.16.clone.sin_hbm, bf16[128,256]{1,0:T(8,128)(2,1)} %wq.1, ...), custom_call_target="tpu_custom_call" | custom-call | tf_op jit(solution)/shard_map/pallas_call | solution.py:590
  185.4 1.9 %copy.14 = bf16[128,2048]{1,0:T(8,128)(2,1)} copy(bf16[128,2048]{1,0:T(8,128)(2,1)} %shard_map.118) | data formatting | bytes 1048576

commit v2 on v1

v2 whole, which is shorter than its diff:
```python
import functools

import jax
import jax.numpy as jnp
import numpy as np
from jax import lax
from jax.experimental import pallas as pl
from jax.experimental.pallas import tpu as pltpu
from jax.sharding import PartitionSpec as P

H = 8
BLOCK = 128
norm_epsilon = 1e-06
group_epsilon = 0.01
MESH = pl.DeviceIdType.MESH
F32 = jnp.float32
BF16 = jnp.bfloat16


def mod(a, n):
    return lax.rem(a + n, n)


def rms(matrix):
    return matrix * lax.rsqrt(jnp.mean(matrix * matrix, axis=-1, keepdims=True) + norm_epsilon)


def silu(v):
    return v / (1.0 + jnp.exp(-v))


def kernel(
    nf,
    nx,
    tok,
    gains,
    lam_ref,
    cos_hbm,
    sin_hbm,
    wq,
    wk,
    wv,
    ws,
    wo,
    wg,
    wu,
    wd,
    out,
    w1,
    w2,
    w3,
    w4,
    xn,
    xw,
    acc,
    qb,
    kb,
    vb,
    gp,
    hid,
    part,
    sib_in,
    stage,
    pass_in,
    from_left,
    from_right,
    am,
    cos,
    sin,
    decay,
    local_sem,
    z_send,
    z_recv,
    y_send,
    y_recv,
    g_send,
    g_recv,
    s_send,
    s_recv,
    r_send,
    r_recv,
):
    rows, width = tok.shape
    seq = xn.shape[0]
    half = width // 2
    quarter = seq // 4
    me = lax.axis_index("fs")
    tp = lax.axis_index("tp")
    group = lax.axis_index("grp")
    x = tp // 2
    core = lax.rem(tp, 2)
    plane = lax.rem(group, 2)
    up = {"fs": mod(me + 1, nf)}
    down = {"fs": mod(me - 1, nf)}
    pair = {"grp": group + 1 - 2 * plane}
    sib = {"tp": 2 * x + 1 - core}
    right = {"tp": 2 * mod(x + 1, nx) + core}
    left = {"tp": 2 * mod(x - 1, nx) + core}

    def copy(src, dst, send, recv, device):
        return pltpu.make_async_remote_copy(
            src_ref=src,
            dst_ref=dst,
            send_sem=send,
            recv_sem=recv,
            device_id=device,
            device_id_type=MESH,
        )

    kd = wq.shape[0]
    mine = pl.ds(pl.multiple_of(me * kd, kd), kd)
    mine_cols = pl.ds(pl.multiple_of(me * kd, kd), kd)
    qw, vw, ff = wq.shape[1], wv.shape[1], wg.shape[1]
    locals_ = [
        (wq, w1.at[mine, 0:qw]),
        (wk, w1.at[mine, qw : 2 * qw]),
        (wv, w1.at[mine, 2 * qw : 2 * qw + vw]),
        (ws, w1.at[mine, 2 * qw + vw : 2 * qw + 2 * vw]),
        (wo, w2.at[:, mine_cols]),
        (wg, w3.at[mine, 0:ff]),
        (wu, w3.at[mine, ff : 2 * ff]),
        (wd, w4.at[:, mine_cols]),
        (cos_hbm, cos),
        (sin_hbm, sin),
    ]
    loads = [
        pltpu.make_async_copy(src, dst, local_sem.at[i]) for i, (src, dst) in enumerate(locals_)
    ]
    for load in loads:
        load.start()

    barrier = pltpu.get_barrier_semaphore()
    for device in (up, down, pair, sib, right, left):
        pl.semaphore_signal(barrier, inc=1, device_id=device, device_id_type=MESH)

    own = pl.multiple_of(tp * rows, rows)

    def norm_in(i, carry):
        at = pl.multiple_of(i * 16, 16)
        value = rms(tok[pl.ds(at, 16), :].astype(F32)) * gains[0:1, :]
        xn[pl.ds(own + at, 16), :] = value.astype(BF16)
        return carry

    lax.fori_loop(0, rows // 16, norm_in, 0)
    pl.semaphore_wait(barrier, 6)

    def third(total):
        return total // 3 // 16 * 16 + (16 if total // 3 % 16 else 0)

    pieces = (4, 2, 2, 2)
    owns = (2, 1, 1, 1)

    def place(a, owner, piece, plane_, rows_half=None):
        ref = (w1, w2, w3, w4)[a]
        if a in (0, 2):
            w = ref.shape[1] // 3 // owns[a]
            start, count = owner * kd, kd
            if rows_half is not None:
                count = kd // 2
                start = start + rows_half * count
            r = pl.ds(pl.multiple_of(start, kd // 2), count)
            if piece < owns[a]:
                at = pl.multiple_of(plane_ * 2 * w * owns[a] + piece * w, 128)
            else:
                at = piece * w
            return ref.at[r, pl.ds(at, w)]
        t = third(ref.shape[0])
        mid = ref.shape[0] - 2 * t
        r = pl.ds(pl.multiple_of(plane_ * (t + mid), 16), t) if piece == 0 else pl.ds(t, mid)
        return ref.at[r, pl.ds(pl.multiple_of(owner * kd, kd), kd)]

    def z_index(a, d, piece):
        return 2 * sum(pieces[:a]) + d * pieces[a] + piece

    def y_index(a, d, piece):
        return 2 * sum(owns[:a]) + d * owns[a] + piece

    def owner_of(d, s):
        return mod(me - s, nf) if d == 0 else lax.rem(me + s, nf)

    far = nf // 2

    def z_copy(a, d, piece, s, rows_half=None):
        src = place(a, owner_of(d, s - 1), piece, plane, rows_half)
        k = z_index(a, d, piece)
        return copy(src, src, z_send.at[k], z_recv.at[k, s - 1], up if d == 0 else down)

    def z_arrived(a, d, piece, s, rows_half=None):
        dst = place(a, owner_of(d, s), piece, plane, rows_half)
        k = z_index(a, d, piece)
        copy(dst, dst, z_send.at[k], z_recv.at[k, s - 1], up if d == 0 else down).wait_recv()

    def y_copy(a, d, piece, s, rows_half=None):
        src = place(a, owner_of(d, s), piece, plane, rows_half)
        k = y_index(a, d, piece)
        return copy(src, src, y_send.at[k], y_recv.at[k, s - 1], pair)

    def y_arrived(a, d, piece, s, rows_half=None):
        dst = place(a, owner_of(d, s), piece, 1 - plane, rows_half)
        k = y_index(a, d, piece)
        copy(dst, dst, y_send.at[k], y_recv.at[k, s - 1], pair).wait_recv()

    def last_half(a, d):
        return d if a in (0, 2) else None

    def has_last(a, d):
        return a in (0, 2) or (a == 1 and d == 0) or (a == 3 and d == 1)

    def begin(a):
        for piece in range(pieces[a]):
            for d in (0, 1):
                z_copy(a, d, piece, 1).start()

    def forward(a, s, piece):
        for d in (0, 1):
            here = s < far or has_last(a, d)
            part_of = last_half(a, d) if s == far else None
            if here:
                z_arrived(a, d, piece, s, part_of)
                z_copy(a, d, piece, s, part_of).wait_send()
            if s < far - 1:
                z_copy(a, d, piece, s + 1).start()
            elif s == far - 1 and has_last(a, d):
                z_copy(a, d, piece, far, last_half(a, d)).start()
            if piece < owns[a]:
                if s > 1:
                    y_copy(a, d, piece, s - 1).wait_send()
                if here:
                    y_copy(a, d, piece, s, part_of).start()

    def slot(*items):
        for piece in range(4):
            for a, s in items:
                if piece < pieces[a]:
                    forward(a, s, piece)

    def y_all(a, s):
        for piece in range(owns[a]):
            for d in (0, 1):
                if s < far or has_last(a, d):
                    y_arrived(a, d, piece, s, last_half(a, d) if s == far else None)

    def y_drain(a):
        for piece in range(owns[a]):
            for d in (0, 1):
                if has_last(a, d):
                    y_copy(a, d, piece, far, last_half(a, d)).wait_send()

    def gather(n, ref, at, count):
        at_left, at_right, at_far = mod(x - 1, nx), mod(x + 1, nx), mod(x + 2, nx)
        lo, hi = pl.ds(0, half), pl.ds(half, half)
        every = pl.ds(0, width)

        def whole(xx, cc, cols=every):
            return ref.at[pl.ds(pl.multiple_of((2 * xx + cc) * rows + at, count), count), cols]

        def send(k, xx, cols, device):
            src = whole(xx, core, cols)
            return copy(src, src, g_send.at[n, k], g_recv.at[n, k], device)

        def arrived(k, xx, cc, cols):
            dst = whole(xx, cc, cols)
            copy(dst, dst, g_send.at[n, k], g_recv.at[n, k], sib).wait_recv()

        sends = []

        def go(*args):
            s = send(*args)
            s.start()
            sends.append(s)

        def first():
            go(1, x, every, right)
            go(2, x, every, left)
            go(0, x, every, sib)

        def second():
            arrived(1, at_left, core, every)
            go(3, at_left, lo, right)
            go(4, at_left, every, sib)
            arrived(2, at_right, core, every)
            go(5, at_right, hi, left)
            go(6, at_right, every, sib)

        def third_():
            arrived(3, at_far, core, lo)
            go(7, at_far, lo, sib)
            arrived(5, at_far, core, hi)
            go(8, at_far, hi, sib)

        def own_chip():
            arrived(0, x, 1 - core, every)

        def near():
            arrived(4, at_left, 1 - core, every)
            arrived(6, at_right, 1 - core, every)

        def rest():
            arrived(7, at_far, 1 - core, lo)
            arrived(8, at_far, 1 - core, hi)

        def drain():
            for s in sends:
                s.wait_send()

        return first, second, third_, own_chip, near, rest, drain

    for load in loads[:4]:
        load.wait()
    begin(0)
    first, second, third_, own_chip, near, rest, drain1 = gather(0, xn, 0, rows)
    first()

    lam = lam_ref[0:1, 0:1]
    dn = lax.broadcasted_iota(jnp.int32, decay.shape, 0) + (seq - quarter)
    dm = lax.broadcasted_iota(jnp.int32, decay.shape, 1)
    dist = (dn - dm).astype(F32)
    decay[...] = jnp.where(dist >= 0.0, jnp.exp(lam * jnp.maximum(dist, 0.0)), 0.0)
    for load in loads[4:]:
        load.wait()

    def k_slice(owner):
        return pl.ds(pl.multiple_of(owner * kd, kd), kd)

    def tiled(tiles, body):
        n = acc.shape[1] // 2

        def step(i, carry):
            r = pl.ds(pl.multiple_of(i // 2 * quarter, quarter), quarter)
            body(r, pl.ds(pl.multiple_of(lax.rem(i, 2) * n, n), n))
            return carry

        lax.fori_loop(2 * tiles[0], 2 * tiles[1], step, 0)

    def add_own(tiles):
        def body(r, c):
            acc[r, c] = jnp.dot(
                xn[r, k_slice(me)], w1[k_slice(me), c], preferred_element_type=F32
            )

        tiled(tiles, body)

    def add_two(s, tiles):
        a, b = k_slice(owner_of(0, s)), k_slice(owner_of(1, s))

        def body(r, c):
            acc[r, c] = (
                acc[r, c]
                + jnp.dot(xn[r, a], w1[a, c], preferred_element_type=F32)
                + jnp.dot(xn[r, b], w1[b, c], preferred_element_type=F32)
            )

        tiled(tiles, body)

    def slot_and_add(s, add):
        forward(0, s, 0)
        forward(1, s, 0)
        add((0, 1))
        forward(0, s, 1)
        add((1, 2))
        forward(0, s, 2)
        forward(1, s, 1)
        add((2, 3))
        forward(0, s, 3)
        add((3, 4))

    begin(1)
    slot((0, 1), (1, 1))
    second()
    slot((0, 2), (1, 2))
    own_chip()
    third_()
    near()
    rest()
    slot_and_add(3, add_own)
    y_all(0, 1)
    slot_and_add(4, functools.partial(add_two, 1))

    for s in (5, 6, 7):
        y_all(0, s - 3)
        slot_and_add(s, functools.partial(add_two, s - 3))
    begin(2)
    begin(3)
    y_all(0, far - 3)
    add_two(far - 3, (0, 4))
    slot((0, far), (1, far))
    y_all(0, far - 2)
    add_two(far - 2, (0, 4))
    y_all(0, far - 1)
    add_two(far - 1, (0, 4))
    y_all(0, far)
    far_slice = k_slice(owner_of(0, far))

    key_scale = float(qw) ** -0.5
    hq = qw // 2

    def finish(i, carry):
        r = pl.ds(pl.multiple_of(i * quarter, quarter), quarter)
        total = acc[r, :] + jnp.dot(xn[r, far_slice], w1[far_slice, :], preferred_element_type=F32)
        c, s = cos[r, :], sin[r, :]
        for ref, at, scale in ((qb, 0, None), (kb, qw, key_scale)):
            a, b = total[:, at : at + hq], total[:, at + hq : at + qw]
            first_half = a * c - b * s
            second_half = a * s + b * c
            if scale is not None:
                first_half, second_half = first_half * scale, second_half * scale
            ref[r, 0:hq] = first_half.astype(BF16)
            ref[r, hq:qw] = second_half.astype(BF16)
        vb[r, :] = total[:, 2 * qw : 2 * qw + vw].astype(BF16)
        acc[r, 2 * qw + vw :] = total[:, 2 * qw + vw :]
        return carry

    lax.fori_loop(0, 4, finish, 0)
    slot((2, 1), (3, 1))

    def retain(i):
        r = slice(i * quarter, (i + 1) * quarter)
        seen = (i + 1) * quarter
        scores = lax.dot_general(
            qb[r, :], kb[0:seen, :], (((1,), (1,)), ((), ())), preferred_element_type=F32
        )
        weighted = (scores * decay[:, seq - seen :]).astype(BF16)
        retained = jnp.dot(weighted, vb[0:seen, :], preferred_element_type=F32)
        centred = retained - jnp.mean(retained, axis=-1, keepdims=True)
        normalized = centred * lax.rsqrt(
            jnp.mean(centred * centred, axis=-1, keepdims=True) + group_epsilon
        )
        gp[r, :] = (silu(acc[r, 2 * qw + vw :]) * normalized).astype(BF16)

    retain(0)
    retain(1)
    retain(2)
    retain(3)
    for s in range(1, far + 1):
        y_all(1, s)
    slot((2, 2), (3, 2))

    lo, hi = slice(0, half), slice(half, width)
    chunk = rows // 2
    near_x = (mod(x + 2, nx), mod(x + 1, nx), mod(x - 1, nx), x)

    class Reduce:
        def __init__(self, n, lhs, weight):
            self.n, self.lhs, self.weight = n, lhs, weight
            self.sends, self.sib, self.got = [], {}, {}

        def project(self, k):
            n, xx = self.n, near_x[k]
            r = pl.ds(pl.multiple_of(2 * xx * rows, 2 * rows), 2 * rows)
            cols = width // 4

            def body(j, carry):
                at = pl.ds(pl.multiple_of(j * cols, cols), cols)
                product = jnp.dot(self.lhs[r, :], self.weight[:, at], preferred_element_type=F32)
                part[r, at] = product.astype(BF16)
                return carry

            lax.fori_loop(0, 4, body, 0)
            s = copy(
                part.at[pl.ds(pl.multiple_of((2 * xx + 1 - core) * rows, rows), rows), :],
                sib_in.at[n, k],
                s_send.at[n, k],
                s_recv.at[n, k],
                sib,
            )
            s.start()
            self.sends.append(s)
            self.sib[k] = s

        def paired(self, k):
            self.sib[k].wait_recv()

        def pre(self, k, ch, cols):
            at = pl.multiple_of((2 * near_x[k] + core) * rows + ch * chunk, chunk)
            r = slice(ch * chunk, (ch + 1) * chunk)
            return part[pl.ds(at, chunk), cols].astype(F32) + sib_in[self.n, k, r, cols].astype(F32)

        def ship(self, name, ch, slot_, value, cols, dst, device):
            n = self.n
            i = ch * 6 + ("pr", "pl", "dr", "dl", "sr", "sl").index(name)
            r = pl.ds(ch * chunk, chunk)
            stage[n, slot_, r, cols] = value.astype(BF16)
            s = copy(stage.at[n, slot_, r, cols], dst, r_send.at[n, i], r_recv.at[n, i], device)
            s.start()
            self.sends.append(s)
            self.got[name, ch] = s

        def passes(self, ch):
            n, r = self.n, pl.ds(ch * chunk, chunk)
            self.ship("pr", ch, 0, self.pre(0, ch, hi), hi, pass_in.at[n, 0, r], right)
            self.ship("pl", ch, 0, self.pre(0, ch, lo), lo, pass_in.at[n, 1, r], left)

        def direct_right(self, ch):
            dst = from_left.at[self.n, pl.ds(ch * chunk, chunk), lo]
            self.ship("dr", ch, 1, self.pre(1, ch, lo), lo, dst, right)

        def direct_left(self, ch):
            dst = from_right.at[self.n, pl.ds(ch * chunk, chunk), hi]
            self.ship("dl", ch, 2, self.pre(2, ch, hi), hi, dst, left)

        def sums(self, ch):
            n, r = self.n, pl.ds(ch * chunk, chunk)
            self.got["pr", ch].wait_recv()
            value = self.pre(1, ch, hi) + pass_in[n, 0, r].astype(F32)
            self.ship("sr", ch, 1, value, hi, from_left.at[n, r, hi], right)
            self.got["pl", ch].wait_recv()
            value = self.pre(2, ch, lo) + pass_in[n, 1, r].astype(F32)
            self.ship("sl", ch, 2, value, lo, from_right.at[n, r, lo], left)

        def arrive(self, ch):
            for name in ("dr", "dl", "sr", "sl"):
                self.got[name, ch].wait_recv()

        def total(self, at, count):
            n, r = self.n, pl.ds(at, count)
            base = pl.multiple_of((2 * x + core) * rows + at, count)
            return (
                (part[pl.ds(base, count), :].astype(F32) + sib_in[n, 3, r, :].astype(F32))
                + from_left[n, r, :].astype(F32)
                + from_right[n, r, :].astype(F32)
            )

        def drain(self):
            for s in self.sends:
                s.wait_send()

    one = Reduce(0, gp, w2)
    one.project(0)
    one.project(1)
    one.paired(0)
    one.passes(0)
    one.passes(1)
    one.project(2)
    one.paired(1)
    one.direct_right(0)
    one.direct_right(1)
    one.project(3)
    one.paired(2)
    one.direct_left(0)
    one.direct_left(1)
    slot((2, 3), (3, 3))
    one.sums(0)
    slot((2, 4), (3, 4))
    one.sums(1)
    one.paired(3)
    slot((2, 5), (3, 5))

    def mixed(i, carry):
        at = pl.multiple_of(i * 16, 16)
        after = tok[pl.ds(at, 16), :].astype(F32) + rms(one.total(at, 16)) * gains[1:2, :]
        am[pl.ds(at, 16), :] = after
        xw[pl.ds(pl.multiple_of(own + at, 16), 16), :] = (rms(after) * gains[2:3, :]).astype(BF16)
        return carry

    per = chunk // 16
    two = [gather(1, xw, 0, chunk), gather(2, xw, chunk, chunk)]
    one.arrive(0)
    lax.fori_loop(0, per, mixed, 0)
    two[0][0]()
    slot((2, 6), (3, 6))
    one.arrive(1)
    lax.fori_loop(per, 2 * per, mixed, 0)
    two[1][0]()
    slot((2, 7), (3, 7))
    two[0][1]()
    slot((2, 8), (3, 8))
    two[1][1]()
    one.drain()
    for s in range(1, far + 1):
        y_all(2, s)

    def feed(k):
        r = pl.ds(pl.multiple_of(2 * near_x[k] * rows, 2 * rows), 2 * rows)
        both = jnp.dot(xw[r, :], w3[...], preferred_element_type=F32)
        hid[r, :] = (silu(both[:, 0:ff]) * both[:, ff:]).astype(BF16)

    two[0][3]()
    two[1][3]()
    feed(3)
    for s in range(1, far + 1):
        y_all(3, s)
    last_one = Reduce(1, hid, w4)
    two[0][4]()
    two[1][4]()
    feed(1)
    last_one.project(1)
    two[0][2]()
    feed(2)
    last_one.project(2)
    last_one.paired(1)
    last_one.direct_right(0)
    last_one.direct_right(1)
    last_one.paired(2)
    last_one.direct_left(0)
    last_one.direct_left(1)
    two[1][2]()
    last_one.project(3)
    two[0][5]()
    two[1][5]()
    feed(0)
    last_one.project(0)
    last_one.paired(0)
    last_one.passes(0)
    last_one.passes(1)
    last_one.paired(3)
    last_one.sums(0)
    last_one.sums(1)

    def last(i, carry):
        at = pl.multiple_of(i * 16, 16)
        r = pl.ds(at, 16)
        out[r, :] = (am[r, :] + rms(last_one.total(at, 16)) * gains[3:4, :]).astype(BF16)
        return carry

    last_one.arrive(0)
    lax.fori_loop(0, per, last, 0)
    last_one.arrive(1)
    lax.fori_loop(per, 2 * per, last, 0)
    drain1()
    two[0][6]()
    two[1][6]()
    last_one.drain()
    for a in range(4):
        y_drain(a)


def layer(nf, nx, tokens, gains, wq, wk, wv, ws, wo, wg, wu, wd):
    rows, width = tokens.shape
    seq = rows * 2 * nx
    qw, vw, ff = wq.shape[1], wv.shape[1], wg.shape[1]
    frequency = 10000.0 ** (-np.linspace(0.0, 1.0, qw // 2))
    angles = np.arange(seq, dtype=np.float64)[:, None] * frequency[None, :]
    cos = jnp.asarray(np.cos(angles).astype(np.float32))
    sin = jnp.asarray(np.sin(angles).astype(np.float32))
    head = lax.axis_index("tp").astype(F32)
    lam = -(4.0 / BLOCK) * (BLOCK / (32.0 * seq)) ** (head / (H - 1))
    lam = jnp.full((8, 128), lam, F32)
    vmem = pl.BlockSpec(memory_space=pltpu.VMEM)
    hbm = pl.BlockSpec(memory_space=pl.ANY)
    dma = pltpu.SemaphoreType.DMA
    far = nf // 2
    half = width // 2
    n1 = 2 * qw + 2 * vw
    return pl.pallas_call(
        functools.partial(kernel, nf, nx),
        out_shape=jax.ShapeDtypeStruct((rows, width), BF16),
        in_specs=[vmem] * 3 + [hbm] * 10,
        out_specs=vmem,
        scratch_shapes=[
            pltpu.VMEM((width, n1), BF16),
            pltpu.VMEM((wo.shape[0], width), BF16),
            pltpu.VMEM((width, 2 * ff), BF16),
            pltpu.VMEM((wd.shape[0], width), BF16),
            pltpu.VMEM((seq, width), BF16),
            pltpu.VMEM((seq, width), BF16),
            pltpu.VMEM((seq, n1), F32),
            pltpu.VMEM((seq, qw), BF16),
            pltpu.VMEM((seq, qw), BF16),
            pltpu.VMEM((seq, vw), BF16),
            pltpu.VMEM((seq, vw), BF16),
            pltpu.VMEM((seq, ff), BF16),
            pltpu.VMEM((seq, width), BF16),
            pltpu.VMEM((2, nx, rows, width), BF16),
            pltpu.VMEM((2, 3, rows, width), BF16),
            pltpu.VMEM((2, 2, rows, half), BF16),
            pltpu.VMEM((2, rows, width), BF16),
            pltpu.VMEM((2, rows, width), BF16),
            pltpu.VMEM((rows, width), F32),
            pltpu.VMEM((seq, qw // 2), F32),
            pltpu.VMEM((seq, qw // 2), F32),
            pltpu.VMEM((seq // 4, seq), F32),
            dma((10,)),
            dma((20,)),
            dma((20, far)),
            dma((10,)),
            dma((10, far)),
            dma((3, 9)),
            dma((3, 9)),
            dma((2, 4)),
            dma((2, 4)),
            dma((2, 12)),
            dma((2, 12)),
        ],
        compiler_params=pltpu.CompilerParams(
            collective_id=0, has_side_effects=True, vmem_limit_bytes=66_000_000
        ),
    )(tokens, gains, lam, cos, sin, wq, wk, wv, ws, wo, wg, wu, wd)


def solution(mesh):
    placed = (
        P(("grp", "fs", "tp"), None),
        P(),
        P("fs", "tp"),
        P("fs", "tp"),
        P("fs", "tp"),
        P("fs", "tp"),
        P("tp", "fs"),
        P("fs", "tp"),
        P("fs", "tp"),
        P("tp", "fs"),
    )
    nf, nt = mesh.shape["fs"], mesh.shape["tp"]
    assert mesh.shape["grp"] % 2 == 0 and nt == 8 and nf % 2 == 0
    return jax.shard_map(
        functools.partial(layer, nf, nt // 2),
        mesh=mesh,
        in_specs=placed,
        out_specs=P(("grp", "fs", "tp"), None),
        check_vma=False,
    )
```

time: 187 us -> 170 us (0.909)
  Pallas kernels: 185 us -> 167 us
    pallas_call x1, Pallas kernels: 185 us -> 167 us  [layer(): pl.pallas_call(functools.partial(kernel, nf, nx), out_shape=jax.ShapeDtyp...]
where the time goes in v2:
time: 170 us
  Pallas kernels  167 us (98%)
  local copies, waits for them, and re-layouts  2.48 us (1%)
    pallas_call x1, Pallas kernels, layer(): pl.pallas_call(functools.partial(kernel, nf, nx), out_shape=jax.ShapeDtyp...  167 us

profile of v2, /device:TPU:33, one launch (start us, length us, event | category | flops | bytes accessed | tf_op | source)
XLA Modules:
  0.0 169.9 jit_solution(2456755409463743595)
XLA Ops:
  0.0 0.6 broadcast_in_dim.3.lam_ref
  0.6 167.3 %shard_map.118 = bf16[128,2048]{1,0:T(8,128)(2,1)} custom-call(bf16[128,2048]{1,0:T(8,128)(2,1)} %tok.1, f32[4,2048]{1,0:T(4,128)} %gains.1, f32[8,128]{1,0:T(8,128)} %broadcast_in_dim.3.lam_ref, f32[1024,128]{1,0:T(8,128)} %constant.15.clone.cos_hbm, f32[1024,128]{1,0:T(8,128)} %constant.16.clone.sin_hbm, bf16[128,256]{1,0:T(8,128)(2,1)} %wq.1, ...), custom_call_target="tpu_custom_call" | custom-call | tf_op jit(solution)/shard_map/pallas_call | solution.py:644
  168.0 1.9 %copy.14 = bf16[128,2048]{1,0:T(8,128)(2,1)} copy(bf16[128,2048]{1,0:T(8,128)(2,1)} %shard_map.118) | data formatting | bytes 1048576

commit v3 on v2

--- a/solution.py
+++ b/solution.py
@@ -35,8 +35,8 @@
     tok,
     gains,
     lam_ref,
-    cos_hbm,
-    sin_hbm,
+    turn_hbm,
+    base_ref,
     wq,
     wk,
     wv,
@@ -65,8 +65,7 @@
     from_left,
     from_right,
     am,
-    cos,
-    sin,
+    turn,
     decay,
     local_sem,
     z_send,
@@ -120,8 +119,7 @@
         (wg, w3.at[mine, 0:ff]),
         (wu, w3.at[mine, ff : 2 * ff]),
         (wd, w4.at[:, mine_cols]),
-        (cos_hbm, cos),
-        (sin_hbm, sin),
+        (turn_hbm, turn),
     ]
     loads = [
         pltpu.make_async_copy(src, dst, local_sem.at[i]) for i, (src, dst) in enumerate(locals_)
@@ -190,15 +188,12 @@
         k = z_index(a, d, piece)
         copy(dst, dst, z_send.at[k], z_recv.at[k, s - 1], up if d == 0 else down).wait_recv()
 
+    def y_sem(a, d, s):
+        return y_recv.at[d * far + s - 1] if a == 0 else y_recv.at[2 * far + a - 1]
+
     def y_copy(a, d, piece, s, rows_half=None):
         src = place(a, owner_of(d, s), piece, plane, rows_half)
-        k = y_index(a, d, piece)
-        return copy(src, src, y_send.at[k], y_recv.at[k, s - 1], pair)
-
-    def y_arrived(a, d, piece, s, rows_half=None):
-        dst = place(a, owner_of(d, s), piece, 1 - plane, rows_half)
-        k = y_index(a, d, piece)
-        copy(dst, dst, y_send.at[k], y_recv.at[k, s - 1], pair).wait_recv()
+        return copy(src, src, y_send.at[y_index(a, d, piece)], y_sem(a, d, s), pair)
 
     def last_half(a, d):
         return d if a in (0, 2) else None
@@ -234,11 +229,25 @@
                 if piece < pieces[a]:
                     forward(a, s, piece)
 
-    def y_all(a, s):
-        for piece in range(owns[a]):
-            for d in (0, 1):
-                if s < far or has_last(a, d):
-                    y_arrived(a, d, piece, s, last_half(a, d) if s == far else None)
+    def y_step(s):
+        w = w1.shape[1] // 3
+        for d in (0, 1):
+            count = kd if s < far else kd // 2
+            start = owner_of(d, s) * kd + (0 if s < far else d * count)
+            at = pl.multiple_of((1 - plane) * 2 * w, 128)
+            dst = w1.at[pl.ds(pl.multiple_of(start, kd // 2), count), pl.ds(at, w)]
+            copy(dst, dst, y_send.at[0], y_sem(0, d, s), pair).wait_recv()
+
+    def y_whole(a):
+        ref = (w1, w2, w3, w4)[a]
+        n = (nf - 1) * kd
+        if a == 2:
+            w = ref.shape[1] // 3
+            dst = ref.at[0:n, pl.ds(pl.multiple_of((1 - plane) * 2 * w, 128), w)]
+        else:
+            t = third(ref.shape[0])
+            dst = ref.at[pl.ds(pl.multiple_of((1 - plane) * (ref.shape[0] - t), 16), t), 0:n]
+        copy(dst, dst, y_send.at[0], y_sem(a, 0, 1), pair).wait_recv()
 
     def y_drain(a):
         for piece in range(owns[a]):
@@ -311,7 +320,7 @@
     first, second, third_, own_chip, near, rest, drain1 = gather(0, xn, 0, rows)
     first()
 
-    lam = lam_ref[0:1, 0:1]
+    lam = lam_ref[pl.ds(tp, 1), 0:1]
     dn = lax.broadcasted_iota(jnp.int32, decay.shape, 0) + (seq - quarter)
     dm = lax.broadcasted_iota(jnp.int32, decay.shape, 1)
     dist = (dn - dm).astype(F32)
@@ -352,43 +361,57 @@
 
         tiled(tiles, body)
 
-    def slot_and_add(s, add):
-        forward(0, s, 0)
+    def slot_and_add(s, adds):
+        for piece in range(4):
+            forward(0, s, piece)
+            if piece < 3:
+                for waits, add, tiles in adds[piece]:
+                    if waits:
+                        y_step(waits)
+                    add(tiles)
         forward(1, s, 0)
-        add((0, 1))
-        forward(0, s, 1)
-        add((1, 2))
-        forward(0, s, 2)
         forward(1, s, 1)
-        add((2, 3))
-        forward(0, s, 3)
-        add((3, 4))
+
+    polls = [(s, piece) for s in range(1, far + 1) for piece in (0, 1)]
+
+    def poll():
+        s, piece = polls.pop(0)
+        forward(2, s, piece)
+        forward(3, s, piece)
+
+    def two_of(s, tiles, wait=True):
+        return s if wait else 0, functools.partial(add_two, s), tiles
 
     begin(1)
-    slot((0, 1), (1, 1))
+    slot((0, 1))
+    forward(1, 1, 0)
+    forward(1, 1, 1)
     second()
-    slot((0, 2), (1, 2))
+    slot((0, 2))
+    forward(1, 2, 0)
+    forward(1, 2, 1)
     own_chip()
     third_()
+    forward(0, 3, 0)
+    forward(0, 3, 1)
     near()
     rest()
-    slot_and_add(3, add_own)
-    y_all(0, 1)
-    slot_and_add(4, functools.partial(add_two, 1))
-
-    for s in (5, 6, 7):
-        y_all(0, s - 3)
-        slot_and_add(s, functools.partial(add_two, s - 3))
+    forward(0, 3, 2)
+    forward(0, 3, 3)
+    forward(1, 3, 0)
+    forward(1, 3, 1)
+    slot_and_add(4, ([(0, add_own, (0, 4))], [two_of(1, (0, 4))], [two_of(2, (0, 2))]))
+    slot_and_add(
+        5, ([two_of(2, (2, 4), False)], [two_of(3, (0, 4))], [two_of(4, (0, 2))])
+    )
+    for s in range(6, far):
+        slot_and_add(s, ([two_of(s - 2, (2, 4), False)], [], [two_of(s - 1, (0, 2))]))
     begin(2)
     begin(3)
-    y_all(0, far - 3)
-    add_two(far - 3, (0, 4))
-    slot((0, far), (1, far))
-    y_all(0, far - 2)
-    add_two(far - 2, (0, 4))
-    y_all(0, far - 1)
-    add_two(far - 1, (0, 4))
-    y_all(0, far)
+    slot_and_add(far, ([two_of(far - 2, (2, 4), False)], [], [two_of(far - 1, (0, 2))]))
+    add_two(far - 1, (2, 4))
+    poll()
+    y_step(far)
     far_slice = k_slice(owner_of(0, far))
 
     key_scale = float(qw) ** -0.5
@@ -397,7 +420,9 @@
     def finish(i, carry):
         r = pl.ds(pl.multiple_of(i * quarter, quarter), quarter)
         total = acc[r, :] + jnp.dot(xn[r, far_slice], w1[far_slice, :], preferred_element_type=F32)
-        c, s = cos[r, :], sin[r, :]
+        cb, sb = base_ref[pl.ds(i, 1), :], base_ref[pl.ds(i + 4, 1), :]
+        c = cb * turn[0] - sb * turn[1]
+        s = sb * turn[0] + cb * turn[1]
         for ref, at, scale in ((qb, 0, None), (kb, qw, key_scale)):
             a, b = total[:, at : at + hq], total[:, at + hq : at + qw]
             first_half = a * c - b * s
@@ -411,64 +436,73 @@
         return carry
 
     lax.fori_loop(0, 4, finish, 0)
-    slot((2, 1), (3, 1))
-
-    def retain(i):
-        r = slice(i * quarter, (i + 1) * quarter)
-        seen = (i + 1) * quarter
+    poll()
+
+    near_x = (mod(x + 2, nx), mod(x + 1, nx), mod(x - 1, nx), x)
+
+    def retain(k):
+        i = near_x[k]
+        r = pl.ds(pl.multiple_of(i * quarter, quarter), quarter)
+        seen = pl.ds(pl.multiple_of((nx - 1 - i) * quarter, quarter), seq)
         scores = lax.dot_general(
-            qb[r, :], kb[0:seen, :], (((1,), (1,)), ((), ())), preferred_element_type=F32
+            qb[r, :], kb[...], (((1,), (1,)), ((), ())), preferred_element_type=F32
         )
-        weighted = (scores * decay[:, seq - seen :]).astype(BF16)
-        retained = jnp.dot(weighted, vb[0:seen, :], preferred_element_type=F32)
+        weighted = (scores * decay[:, seen]).astype(BF16)
+        retained = jnp.dot(weighted, vb[...], preferred_element_type=F32)
         centred = retained - jnp.mean(retained, axis=-1, keepdims=True)
         normalized = centred * lax.rsqrt(
             jnp.mean(centred * centred, axis=-1, keepdims=True) + group_epsilon
         )
         gp[r, :] = (silu(acc[r, 2 * qw + vw :]) * normalized).astype(BF16)
 
-    retain(0)
-    retain(1)
-    retain(2)
-    retain(3)
-    for s in range(1, far + 1):
-        y_all(1, s)
-    slot((2, 2), (3, 2))
-
     lo, hi = slice(0, half), slice(half, width)
     chunk = rows // 2
-    near_x = (mod(x + 2, nx), mod(x + 1, nx), mod(x - 1, nx), x)
+
+    def blocks_of(items):
+        return [
+            pl.ds(pl.multiple_of((2 * near_x[k] + cc) * rows + ch * chunk, chunk), chunk)
+            for k, ch in items
+            for cc in (0, 1)
+        ]
+
+    def load_rows(ref, items):
+        return jnp.concatenate([ref[r, :] for r in blocks_of(items)], axis=0)
 
     class Reduce:
         def __init__(self, n, lhs, weight):
             self.n, self.lhs, self.weight = n, lhs, weight
             self.sends, self.sib, self.got = [], {}, {}
 
-        def project(self, k):
-            n, xx = self.n, near_x[k]
-            r = pl.ds(pl.multiple_of(2 * xx * rows, 2 * rows), 2 * rows)
+        def project(self, *items):
+            n = self.n
             cols = width // 4
 
             def body(j, carry):
                 at = pl.ds(pl.multiple_of(j * cols, cols), cols)
-                product = jnp.dot(self.lhs[r, :], self.weight[:, at], preferred_element_type=F32)
-                part[r, at] = product.astype(BF16)
+                product = jnp.dot(
+                    load_rows(self.lhs, items), self.weight[:, at], preferred_element_type=F32
+                ).astype(BF16)
+                for i, r in enumerate(blocks_of(items)):
+                    part[r, at] = product[i * chunk : (i + 1) * chunk]
                 return carry
 
             lax.fori_loop(0, 4, body, 0)
-            s = copy(
-                part.at[pl.ds(pl.multiple_of((2 * xx + 1 - core) * rows, rows), rows), :],
-                sib_in.at[n, k],
-                s_send.at[n, k],
-                s_recv.at[n, k],
-                sib,
-            )
-            s.start()
-            self.sends.append(s)
-            self.sib[k] = s
-
-        def paired(self, k):
-            self.sib[k].wait_recv()
+            for k, ch in items:
+                i = 2 * k + ch
+                start = pl.multiple_of((2 * near_x[k] + 1 - core) * rows + ch * chunk, chunk)
+                s = copy(
+                    part.at[pl.ds(start, chunk), :],
+                    sib_in.at[n, k, pl.ds(ch * chunk, chunk)],
+                    s_send.at[n, i],
+                    s_recv.at[n, i],
+                    sib,
+                )
+                s.start()
+                self.sends.append(s)
+                self.sib[k, ch] = s
+
+        def paired(self, k, ch):
+            self.sib[k, ch].wait_recv()
 
         def pre(self, k, ch, cols):
             at = pl.multiple_of((2 * near_x[k] + core) * rows + ch * chunk, chunk)
@@ -486,15 +520,18 @@
             self.got[name, ch] = s
 
         def passes(self, ch):
+            self.paired(0, ch)
             n, r = self.n, pl.ds(ch * chunk, chunk)
             self.ship("pr", ch, 0, self.pre(0, ch, hi), hi, pass_in.at[n, 0, r], right)
             self.ship("pl", ch, 0, self.pre(0, ch, lo), lo, pass_in.at[n, 1, r], left)
 
         def direct_right(self, ch):
+            self.paired(1, ch)
             dst = from_left.at[self.n, pl.ds(ch * chunk, chunk), lo]
             self.ship("dr", ch, 1, self.pre(1, ch, lo), lo, dst, right)
 
         def direct_left(self, ch):
+            self.paired(2, ch)
             dst = from_right.at[self.n, pl.ds(ch * chunk, chunk), hi]
             self.ship("dl", ch, 2, self.pre(2, ch, hi), hi, dst, left)
 
@@ -525,25 +562,32 @@
                 s.wait_send()
 
     one = Reduce(0, gp, w2)
-    one.project(0)
-    one.project(1)
-    one.paired(0)
+    retain(0)
+    y_whole(1)
+    one.project((0, 0), (0, 1))
+    poll()
+    retain(1)
     one.passes(0)
     one.passes(1)
-    one.project(2)
-    one.paired(1)
+    one.project((1, 0), (1, 1))
+    poll()
+    retain(2)
+    one.project((2, 0), (2, 1))
     one.direct_right(0)
+    poll()
+    retain(3)
+    one.direct_left(0)
+    one.sums(0)
     one.direct_right(1)
-    one.project(3)
-    one.paired(2)
-    one.direct_left(0)
     one.direct_left(1)
-    slot((2, 3), (3, 3))
-    one.sums(0)
-    slot((2, 4), (3, 4))
+    poll()
+    one.project((3, 0), (3, 1))
+    poll()
     one.sums(1)
-    one.paired(3)
-    slot((2, 5), (3, 5))
+    poll()
+    one.paired(3, 0)
+    one.paired(3, 1)
+    poll()
 
     def mixed(i, carry):
         at = pl.multiple_of(i * 16, 16)
@@ -557,54 +601,58 @@
     one.arrive(0)
     lax.fori_loop(0, per, mixed, 0)
     two[0][0]()
-    slot((2, 6), (3, 6))
+    poll()
+    poll()
     one.arrive(1)
     lax.fori_loop(per, 2 * per, mixed, 0)
     two[1][0]()
-    slot((2, 7), (3, 7))
+    poll()
+    poll()
+    one.drain()
+    poll()
     two[0][1]()
-    slot((2, 8), (3, 8))
-    two[1][1]()
-    one.drain()
-    for s in range(1, far + 1):
-        y_all(2, s)
-
-    def feed(k):
-        r = pl.ds(pl.multiple_of(2 * near_x[k] * rows, 2 * rows), 2 * rows)
-        both = jnp.dot(xw[r, :], w3[...], preferred_element_type=F32)
-        hid[r, :] = (silu(both[:, 0:ff]) * both[:, ff:]).astype(BF16)
-
+    poll()
+    poll()
+    assert not polls
+
+    def feed(*items):
+        both = jnp.dot(load_rows(xw, items), w3[...], preferred_element_type=F32)
+        hidden = (silu(both[:, 0:ff]) * both[:, ff:]).astype(BF16)
+        for i, r in enumerate(blocks_of(items)):
+            hid[r, :] = hidden[i * chunk : (i + 1) * chunk]
+
+    last_one = Reduce(1, hid, w4)
     two[0][3]()
     two[1][3]()
-    feed(3)
-    for s in range(1, far + 1):
-        y_all(3, s)
-    last_one = Reduce(1, hid, w4)
+    y_whole(2)
+    feed((3, 0), (3, 1))
     two[0][4]()
+    feed((1, 0), (2, 0))
+    y_whole(3)
+    last_one.project((1, 0), (2, 0))
+    two[1][1]()
+    last_one.direct_right(0)
+    last_one.direct_left(0)
+    two[0][2]()
     two[1][4]()
-    feed(1)
-    last_one.project(1)
-    two[0][2]()
-    feed(2)
-    last_one.project(2)
-    last_one.paired(1)
-    last_one.direct_right(0)
+    feed((1, 1), (2, 1))
+    last_one.project((1, 1), (2, 1))
+    two[0][5]()
+    feed((0, 0))
+    last_one.project((0, 0))
     last_one.direct_right(1)
-    last_one.paired(2)
-    last_one.direct_left(0)
     last_one.direct_left(1)
     two[1][2]()
-    last_one.project(3)
-    two[0][5]()
+    last_one.passes(0)
     two[1][5]()
-    feed(0)
-    last_one.project(0)
-    last_one.paired(0)
-    last_one.passes(0)
+    feed((0, 1))
+    last_one.project((0, 1))
     last_one.passes(1)
-    last_one.paired(3)
+    last_one.project((3, 0), (3, 1))
     last_one.sums(0)
     last_one.sums(1)
+    last_one.paired(3, 0)
+    last_one.paired(3, 1)
 
     def last(i, carry):
         at = pl.multiple_of(i * 16, 16)
@@ -629,12 +677,13 @@
     seq = rows * 2 * nx
     qw, vw, ff = wq.shape[1], wv.shape[1], wg.shape[1]
     frequency = 10000.0 ** (-np.linspace(0.0, 1.0, qw // 2))
-    angles = np.arange(seq, dtype=np.float64)[:, None] * frequency[None, :]
-    cos = jnp.asarray(np.cos(angles).astype(np.float32))
-    sin = jnp.asarray(np.sin(angles).astype(np.float32))
-    head = lax.axis_index("tp").astype(F32)
-    lam = -(4.0 / BLOCK) * (BLOCK / (32.0 * seq)) ** (head / (H - 1))
-    lam = jnp.full((8, 128), lam, F32)
+    within = np.arange(seq // 4, dtype=np.float64)[:, None] * frequency[None, :]
+    starts = np.arange(4, dtype=np.float64)[:, None] * (seq // 4) * frequency[None, :]
+    turn = jnp.asarray(np.stack([np.cos(within), np.sin(within)]).astype(np.float32))
+    base = jnp.asarray(np.concatenate([np.cos(starts), np.sin(starts)]).astype(np.float32))
+    heads = np.arange(2 * nx, dtype=np.float64)
+    lam = -(4.0 / BLOCK) * (BLOCK / (32.0 * seq)) ** (heads / (H - 1))
+    lam = jnp.asarray(np.repeat(lam[:, None], 128, axis=1).astype(np.float32))
     vmem = pl.BlockSpec(memory_space=pltpu.VMEM)
     hbm = pl.BlockSpec(memory_space=pl.ANY)
     dma = pltpu.SemaphoreType.DMA
@@ -644,7 +693,7 @@
     return pl.pallas_call(
         functools.partial(kernel, nf, nx),
         out_shape=jax.ShapeDtypeStruct((rows, width), BF16),
-        in_specs=[vmem] * 3 + [hbm] * 10,
+        in_specs=[vmem] * 3 + [hbm, vmem] + [hbm] * 8,
         out_specs=vmem,
         scratch_shapes=[
             pltpu.VMEM((width, n1), BF16),
@@ -666,25 +715,24 @@
             pltpu.VMEM((2, rows, width), BF16),
             pltpu.VMEM((2, rows, width), BF16),
             pltpu.VMEM((rows, width), F32),
-            pltpu.VMEM((seq, qw // 2), F32),
-            pltpu.VMEM((seq, qw // 2), F32),
-            pltpu.VMEM((seq // 4, seq), F32),
+            pltpu.VMEM((2, seq // 4, qw // 2), F32),
+            pltpu.VMEM((seq // 4, 2 * seq - seq // 4), F32),
             dma((10,)),
             dma((20,)),
             dma((20, far)),
             dma((10,)),
-            dma((10, far)),
+            dma((2 * far + 3,)),
             dma((3, 9)),
             dma((3, 9)),
-            dma((2, 4)),
-            dma((2, 4)),
+            dma((2, 8)),
+            dma((2, 8)),
             dma((2, 12)),
             dma((2, 12)),
         ],
         compiler_params=pltpu.CompilerParams(
             collective_id=0, has_side_effects=True, vmem_limit_bytes=66_000_000
         ),
-    )(tokens, gains, lam, cos, sin, wq, wk, wv, ws, wo, wg, wu, wd)
+    )(tokens, gains, lam, turn, base, wq, wk, wv, ws, wo, wg, wu, wd)
 
 
 def solution(mesh):

time: 170 us -> 158 us (0.929)
  Pallas kernels: 167 us -> 156 us
    pallas_call x1, Pallas kernels: 167 us -> 156 us  [layer(): pl.pallas_call(functools.partial(kernel, nf, nx), out_shape=jax.ShapeDtyp...]
where the time goes in v3:
time: 158 us
  Pallas kernels  156 us (99%)
  local copies, waits for them, and re-layouts  1.88 us (1%)
    pallas_call x1, Pallas kernels, layer(): pl.pallas_call(functools.partial(kernel, nf, nx), out_shape=jax.ShapeDtyp...  156 us

profile of v3, /device:TPU:33, one launch (start us, length us, event | category | flops | bytes accessed | tf_op | source)
XLA Modules:
  0.0 157.6 jit_solution(5661846492431084925)
XLA Ops:
  0.0 155.7 %shard_map.127 = bf16[128,2048]{1,0:T(8,128)(2,1)} custom-call(bf16[128,2048]{1,0:T(8,128)(2,1)} %tok.1, f32[4,2048]{1,0:T(4,128)} %gains.1, f32[8,128]{1,0:T(8,128)} %constant.8.clone.lam_ref, f32[2,256,128]{2,1,0:T(8,128)} %constant.6.clone.turn_hbm, f32[8,128]{1,0:T(8,128)} %constant.7.clone.base_ref, bf16[128,256]{1,0:T(8,128)(2,1)} %wq.1, ...), custom_call_target="tpu_custom_call" | custom-call | tf_op jit(solution)/shard_map/pallas_call | solution.py:693
  155.7 1.9 %copy.15 = bf16[128,2048]{1,0:T(8,128)(2,1)} copy(bf16[128,2048]{1,0:T(8,128)(2,1)} %shard_map.127) | data formatting | bytes 1048576

commit v4 on v3

--- a/solution.py
+++ b/solution.py
@@ -32,11 +32,11 @@
 def kernel(
     nf,
     nx,
-    tok,
-    gains,
-    lam_ref,
+    tok_hbm,
+    gains_hbm,
+    lam_hbm,
     turn_hbm,
-    base_ref,
+    base_hbm,
     wq,
     wk,
     wv,
@@ -67,6 +67,10 @@
     am,
     turn,
     decay,
+    tok,
+    gains,
+    lam_ref,
+    base_ref,
     local_sem,
     z_send,
     z_recv,
@@ -120,11 +124,15 @@
         (wu, w3.at[mine, ff : 2 * ff]),
         (wd, w4.at[:, mine_cols]),
         (turn_hbm, turn),
+        (lam_hbm, lam_ref),
+        (base_hbm, base_ref),
+        (tok_hbm, tok),
+        (gains_hbm, gains),
     ]
     loads = [
         pltpu.make_async_copy(src, dst, local_sem.at[i]) for i, (src, dst) in enumerate(locals_)
     ]
-    for load in loads:
+    for load in loads[-2:] + loads[:-2]:
         load.start()
 
     barrier = pltpu.get_barrier_semaphore()
@@ -139,14 +147,16 @@
         xn[pl.ds(own + at, 16), :] = value.astype(BF16)
         return carry
 
+    for load in loads[-2:]:
+        load.wait()
     lax.fori_loop(0, rows // 16, norm_in, 0)
     pl.semaphore_wait(barrier, 6)
 
-    def third(total):
-        return total // 3 // 16 * 16 + (16 if total // 3 % 16 else 0)
-
-    pieces = (4, 2, 2, 2)
-    owns = (2, 1, 1, 1)
+    def shared(a):
+        return w2.shape[0] // 4 if a == 1 else w4.shape[0] // 3
+
+    pieces = (4, 2, 4, 2)
+    owns = (2, 1, 2, 1)
 
     def place(a, owner, piece, plane_, rows_half=None):
         ref = (w1, w2, w3, w4)[a]
@@ -162,11 +172,13 @@
             else:
                 at = piece * w
             return ref.at[r, pl.ds(at, w)]
-        t = third(ref.shape[0])
+        t = shared(a)
         mid = ref.shape[0] - 2 * t
         r = pl.ds(pl.multiple_of(plane_ * (t + mid), 16), t) if piece == 0 else pl.ds(t, mid)
         return ref.at[r, pl.ds(pl.multiple_of(owner * kd, kd), kd)]
 
+    half_streams = 2 * (pieces[0] + pieces[1])
+
     def z_index(a, d, piece):
         return 2 * sum(pieces[:a]) + d * pieces[a] + piece
 
@@ -181,12 +193,12 @@
     def z_copy(a, d, piece, s, rows_half=None):
         src = place(a, owner_of(d, s - 1), piece, plane, rows_half)
         k = z_index(a, d, piece)
-        return copy(src, src, z_send.at[k], z_recv.at[k, s - 1], up if d == 0 else down)
+        return copy(src, src, z_send.at[k], z_recv.at[k % half_streams, s - 1], up if d == 0 else down)
 
     def z_arrived(a, d, piece, s, rows_half=None):
         dst = place(a, owner_of(d, s), piece, plane, rows_half)
         k = z_index(a, d, piece)
-        copy(dst, dst, z_send.at[k], z_recv.at[k, s - 1], up if d == 0 else down).wait_recv()
+        copy(dst, dst, z_send.at[k], z_recv.at[k % half_streams, s - 1], up if d == 0 else down).wait_recv()
 
     def y_sem(a, d, s):
         return y_recv.at[d * far + s - 1] if a == 0 else y_recv.at[2 * far + a - 1]
@@ -245,7 +257,7 @@
             w = ref.shape[1] // 3
             dst = ref.at[0:n, pl.ds(pl.multiple_of((1 - plane) * 2 * w, 128), w)]
         else:
-            t = third(ref.shape[0])
+            t = shared(a)
             dst = ref.at[pl.ds(pl.multiple_of((1 - plane) * (ref.shape[0] - t), 16), t), 0:n]
         copy(dst, dst, y_send.at[0], y_sem(a, 0, 1), pair).wait_recv()
 
@@ -265,11 +277,11 @@
 
         def send(k, xx, cols, device):
             src = whole(xx, core, cols)
-            return copy(src, src, g_send.at[n, k], g_recv.at[n, k], device)
+            return copy(src, src, g_send.at[n // 2, k], g_recv.at[n // 2, k], device)
 
         def arrived(k, xx, cc, cols):
             dst = whole(xx, cc, cols)
-            copy(dst, dst, g_send.at[n, k], g_recv.at[n, k], sib).wait_recv()
+            copy(dst, dst, g_send.at[n // 2, k], g_recv.at[n // 2, k], sib).wait_recv()
 
         sends = []
 
@@ -320,13 +332,14 @@
     first, second, third_, own_chip, near, rest, drain1 = gather(0, xn, 0, rows)
     first()
 
+    for load in loads[4:-2]:
+        load.wait()
+
     lam = lam_ref[pl.ds(tp, 1), 0:1]
     dn = lax.broadcasted_iota(jnp.int32, decay.shape, 0) + (seq - quarter)
     dm = lax.broadcasted_iota(jnp.int32, decay.shape, 1)
     dist = (dn - dm).astype(F32)
     decay[...] = jnp.where(dist >= 0.0, jnp.exp(lam * jnp.maximum(dist, 0.0)), 0.0)
-    for load in loads[4:]:
-        load.wait()
 
     def k_slice(owner):
         return pl.ds(pl.multiple_of(owner * kd, kd), kd)
@@ -372,12 +385,20 @@
         forward(1, s, 0)
         forward(1, s, 1)
 
-    polls = [(s, piece) for s in range(1, far + 1) for piece in (0, 1)]
-
-    def poll():
-        s, piece = polls.pop(0)
-        forward(2, s, piece)
-        forward(3, s, piece)
+    order = (((2, 0), (3, 0)), ((2, 1),), ((2, 2), (3, 1)), ((2, 3),))
+    polls = [(s, group) for s in range(1, far + 1) for group in order]
+
+    def poll(count=1):
+        for _ in range(count):
+            s, group = polls.pop(0)
+            for a, piece in group:
+                forward(a, s, piece)
+
+    def begin_polled():
+        for group in order:
+            for a, piece in group:
+                for d in (0, 1):
+                    z_copy(a, d, piece, 1).start()
 
     def two_of(s, tiles, wait=True):
         return s if wait else 0, functools.partial(add_two, s), tiles
@@ -400,17 +421,12 @@
     forward(0, 3, 3)
     forward(1, 3, 0)
     forward(1, 3, 1)
-    slot_and_add(4, ([(0, add_own, (0, 4))], [two_of(1, (0, 4))], [two_of(2, (0, 2))]))
-    slot_and_add(
-        5, ([two_of(2, (2, 4), False)], [two_of(3, (0, 4))], [two_of(4, (0, 2))])
-    )
+    slot_and_add(4, ([(0, add_own, (0, 4))], [two_of(1, (0, 4))], [two_of(2, (0, 4))]))
+    slot_and_add(5, ([two_of(3, (0, 4))], [], [two_of(4, (0, 4))]))
     for s in range(6, far):
-        slot_and_add(s, ([two_of(s - 2, (2, 4), False)], [], [two_of(s - 1, (0, 2))]))
-    begin(2)
-    begin(3)
-    slot_and_add(far, ([two_of(far - 2, (2, 4), False)], [], [two_of(far - 1, (0, 2))]))
-    add_two(far - 1, (2, 4))
-    poll()
+        slot_and_add(s, ([], [], [two_of(s - 1, (0, 4))]))
+    begin_polled()
+    slot_and_add(far, ([], [two_of(far - 1, (0, 2))], [two_of(far - 1, (2, 4), False)]))
     y_step(far)
     far_slice = k_slice(owner_of(0, far))
 
@@ -436,7 +452,7 @@
         return carry
 
     lax.fori_loop(0, 4, finish, 0)
-    poll()
+    poll(2)
 
     near_x = (mod(x + 2, nx), mod(x + 1, nx), mod(x - 1, nx), x)
 
@@ -493,8 +509,8 @@
                 s = copy(
                     part.at[pl.ds(start, chunk), :],
                     sib_in.at[n, k, pl.ds(ch * chunk, chunk)],
-                    s_send.at[n, i],
-                    s_recv.at[n, i],
+                    s_send.at[i],
+                    s_recv.at[i],
                     sib,
                 )
                 s.start()
@@ -514,7 +530,7 @@
             i = ch * 6 + ("pr", "pl", "dr", "dl", "sr", "sl").index(name)
             r = pl.ds(ch * chunk, chunk)
             stage[n, slot_, r, cols] = value.astype(BF16)
-            s = copy(stage.at[n, slot_, r, cols], dst, r_send.at[n, i], r_recv.at[n, i], device)
+            s = copy(stage.at[n, slot_, r, cols], dst, r_send.at[i], r_recv.at[i], device)
             s.start()
             self.sends.append(s)
             self.got[name, ch] = s
@@ -566,28 +582,32 @@
     y_whole(1)
     one.project((0, 0), (0, 1))
     poll()
-    retain(1)
     one.passes(0)
     one.passes(1)
+    retain(1)
+    poll(2)
     one.project((1, 0), (1, 1))
+    poll(2)
+    retain(2)
     poll()
-    retain(2)
     one.project((2, 0), (2, 1))
     one.direct_right(0)
     poll()
     retain(3)
     one.direct_left(0)
+    poll()
     one.sums(0)
     one.direct_right(1)
     one.direct_left(1)
-    poll()
+    poll(2)
     one.project((3, 0), (3, 1))
     poll()
     one.sums(1)
-    poll()
+    poll(3)
     one.paired(3, 0)
     one.paired(3, 1)
-    poll()
+    poll(2)
+    drain1()
 
     def mixed(i, carry):
         at = pl.multiple_of(i * 16, 16)
@@ -601,18 +621,14 @@
     one.arrive(0)
     lax.fori_loop(0, per, mixed, 0)
     two[0][0]()
-    poll()
-    poll()
+    poll(4)
     one.arrive(1)
     lax.fori_loop(per, 2 * per, mixed, 0)
     two[1][0]()
-    poll()
-    poll()
     one.drain()
-    poll()
+    poll(5)
     two[0][1]()
-    poll()
-    poll()
+    poll(5)
     assert not polls
 
     def feed(*items):
@@ -622,31 +638,31 @@
             hid[r, :] = hidden[i * chunk : (i + 1) * chunk]
 
     last_one = Reduce(1, hid, w4)
-    two[0][3]()
-    two[1][3]()
+    two[1][1]()
     y_whole(2)
-    feed((3, 0), (3, 1))
     two[0][4]()
     feed((1, 0), (2, 0))
     y_whole(3)
     last_one.project((1, 0), (2, 0))
-    two[1][1]()
-    last_one.direct_right(0)
-    last_one.direct_left(0)
     two[0][2]()
     two[1][4]()
     feed((1, 1), (2, 1))
+    last_one.direct_right(0)
+    last_one.direct_left(0)
     last_one.project((1, 1), (2, 1))
+    two[1][2]()
     two[0][5]()
     feed((0, 0))
     last_one.project((0, 0))
     last_one.direct_right(1)
     last_one.direct_left(1)
-    two[1][2]()
-    last_one.passes(0)
     two[1][5]()
     feed((0, 1))
+    last_one.passes(0)
     last_one.project((0, 1))
+    two[0][3]()
+    two[1][3]()
+    feed((3, 0), (3, 1))
     last_one.passes(1)
     last_one.project((3, 0), (3, 1))
     last_one.sums(0)
@@ -664,7 +680,6 @@
     lax.fori_loop(0, per, last, 0)
     last_one.arrive(1)
     lax.fori_loop(per, 2 * per, last, 0)
-    drain1()
     two[0][6]()
     two[1][6]()
     last_one.drain()
@@ -693,7 +708,7 @@
     return pl.pallas_call(
         functools.partial(kernel, nf, nx),
         out_shape=jax.ShapeDtypeStruct((rows, width), BF16),
-        in_specs=[vmem] * 3 + [hbm, vmem] + [hbm] * 8,
+        in_specs=[hbm] * 13,
         out_specs=vmem,
         scratch_shapes=[
             pltpu.VMEM((width, n1), BF16),
@@ -717,17 +732,21 @@
             pltpu.VMEM((rows, width), F32),
             pltpu.VMEM((2, seq // 4, qw // 2), F32),
             pltpu.VMEM((seq // 4, 2 * seq - seq // 4), F32),
-            dma((10,)),
-            dma((20,)),
-            dma((20, far)),
-            dma((10,)),
+            pltpu.VMEM(tokens.shape, BF16),
+            pltpu.VMEM(gains.shape, F32),
+            pltpu.VMEM(lam.shape, F32),
+            pltpu.VMEM(base.shape, F32),
+            dma((13,)),
+            dma((24,)),
+            dma((12, far)),
+            dma((12,)),
             dma((2 * far + 3,)),
-            dma((3, 9)),
-            dma((3, 9)),
-            dma((2, 8)),
-            dma((2, 8)),
-            dma((2, 12)),
-            dma((2, 12)),
+            dma((2, 9)),
+            dma((2, 9)),
+            dma((8,)),
+            dma((8,)),
+            dma((12,)),
+            dma((12,)),
         ],
         compiler_params=pltpu.CompilerParams(
             collective_id=0, has_side_effects=True, vmem_limit_bytes=66_000_000

time: 158 us -> 155 us (0.981)
  Pallas kernels: 156 us -> 153 us
    pallas_call x1, Pallas kernels: 156 us -> 153 us  [layer(): pl.pallas_call(functools.partial(kernel, nf, nx), out_shape=jax.ShapeDtyp...]
where the time goes in v4:
time: 155 us
  Pallas kernels  153 us (99%)
  local copies, waits for them, and re-layouts  1.88 us (1%)
    pallas_call x1, Pallas kernels, layer(): pl.pallas_call(functools.partial(kernel, nf, nx), out_shape=jax.ShapeDtyp...  153 us

profile of v4, /device:TPU:33, one launch (start us, length us, event | category | flops | bytes accessed | tf_op | source)
XLA Modules:
  0.0 154.8 jit_solution(15871934816901453858)
XLA Ops:
  0.0 152.9 %shard_map.127 = bf16[128,2048]{1,0:T(8,128)(2,1)} custom-call(bf16[128,2048]{1,0:T(8,128)(2,1)} %tok_hbm.1, f32[4,2048]{1,0:T(4,128)} %gains_hbm.1, f32[8,128]{1,0:T(8,128)} %constant.8.clone.lam_hbm, f32[2,256,128]{2,1,0:T(8,128)} %constant.6.clone.turn_hbm, f32[8,128]{1,0:T(8,128)} %constant.7.clone.base_hbm, bf16[128,256]{1,0:T(8,128)(2,1)} %wq.1, ...), custom_call_target="tpu_custom_call" | custom-call | tf_op jit(solution)/shard_map/pallas_call | solution.py:708
  152.9 1.9 %copy.15 = bf16[128,2048]{1,0:T(8,128)(2,1)} copy(bf16[128,2048]{1,0:T(8,128)(2,1)} %shard_map.127) | data formatting | bytes 1048576

commit v5 on v4

--- a/solution.py
+++ b/solution.py
@@ -388,11 +388,13 @@
     order = (((2, 0), (3, 0)), ((2, 1),), ((2, 2), (3, 1)), ((2, 3),))
     polls = [(s, group) for s in range(1, far + 1) for group in order]
 
+    def pass_on(s, group):
+        for a, piece in group:
+            forward(a, s, piece)
+
     def poll(count=1):
         for _ in range(count):
-            s, group = polls.pop(0)
-            for a, piece in group:
-                forward(a, s, piece)
+            pass_on(*polls.pop(0))
 
     def begin_polled():
         for group in order:
@@ -487,7 +489,7 @@
     class Reduce:
         def __init__(self, n, lhs, weight):
             self.n, self.lhs, self.weight = n, lhs, weight
-            self.sends, self.sib, self.got = [], {}, {}
+            self.sends, self.got = [], {}
 
         def project(self, *items):
             n = self.n
@@ -504,21 +506,20 @@
 
             lax.fori_loop(0, 4, body, 0)
             for k, ch in items:
-                i = 2 * k + ch
-                start = pl.multiple_of((2 * near_x[k] + 1 - core) * rows + ch * chunk, chunk)
-                s = copy(
-                    part.at[pl.ds(start, chunk), :],
-                    sib_in.at[n, k, pl.ds(ch * chunk, chunk)],
-                    s_send.at[i],
-                    s_recv.at[i],
-                    sib,
-                )
-                s.start()
-                self.sends.append(s)
-                self.sib[k, ch] = s
+                self.to_sibling(k, ch).start()
+
+        def to_sibling(self, k, ch):
+            start = pl.multiple_of((2 * near_x[k] + 1 - core) * rows + ch * chunk, chunk)
+            return copy(
+                part.at[pl.ds(start, chunk), :],
+                sib_in.at[self.n, k, pl.ds(ch * chunk, chunk)],
+                s_send.at[2 * k + ch],
+                s_recv.at[2 * k + ch],
+                sib,
+            )
 
         def paired(self, k, ch):
-            self.sib[k, ch].wait_recv()
+            self.to_sibling(k, ch).wait_recv()
 
         def pre(self, k, ch, cols):
             at = pl.multiple_of((2 * near_x[k] + core) * rows + ch * chunk, chunk)
@@ -576,26 +577,43 @@
         def drain(self):
             for s in self.sends:
                 s.wait_send()
+            for k in range(nx):
+                self.to_sibling(k, 0).wait_send()
+                self.to_sibling(k, 1).wait_send()
 
     one = Reduce(0, gp, w2)
     retain(0)
     y_whole(1)
     one.project((0, 0), (0, 1))
     poll()
+    early = [polls.pop(0) for _ in range(4)]
+
+    def neighbours():
+        retain(1)
+        pass_on(*early[0])
+        one.project((1, 0), (1, 1))
+        pass_on(*early[1])
+        retain(2)
+        pass_on(*early[2])
+        one.project((2, 0), (2, 1))
+        pass_on(*early[3])
+
+    @pl.when(core == 1)
+    def _():
+        neighbours()
+
     one.passes(0)
     one.passes(1)
-    retain(1)
-    poll(2)
-    one.project((1, 0), (1, 1))
-    poll(2)
-    retain(2)
-    poll()
-    one.project((2, 0), (2, 1))
+
+    @pl.when(core == 0)
+    def _():
+        neighbours()
+
     one.direct_right(0)
     poll()
+    one.direct_left(0)
     retain(3)
-    one.direct_left(0)
-    poll()
+    poll(2)
     one.sums(0)
     one.direct_right(1)
     one.direct_left(1)

time: 155 us -> 153 us (0.987)
  Pallas kernels: 153 us -> 151 us
    pallas_call x1, Pallas kernels: 153 us -> 151 us  [layer(): pl.pallas_call(functools.partial(kernel, nf, nx), out_shape=jax.ShapeDtyp...]
where the time goes in v5:
time: 153 us
  Pallas kernels  151 us (99%)
  local copies, waits for them, and re-layouts  1.88 us (1%)
    pallas_call x1, Pallas kernels, layer(): pl.pallas_call(functools.partial(kernel, nf, nx), out_shape=jax.ShapeDtyp...  151 us

profile of v5, /device:TPU:33, one launch (start us, length us, event | category | flops | bytes accessed | tf_op | source)
XLA Modules:
  0.0 153.2 jit_solution(18212664386722894972)
XLA Ops:
  0.0 151.3 %shard_map.127 = bf16[128,2048]{1,0:T(8,128)(2,1)} custom-call(bf16[128,2048]{1,0:T(8,128)(2,1)} %tok_hbm.1, f32[4,2048]{1,0:T(4,128)} %gains_hbm.1, f32[8,128]{1,0:T(8,128)} %constant.8.clone.lam_hbm, f32[2,256,128]{2,1,0:T(8,128)} %constant.6.clone.turn_hbm, f32[8,128]{1,0:T(8,128)} %constant.7.clone.base_hbm, bf16[128,256]{1,0:T(8,128)(2,1)} %wq.1, ...), custom_call_target="tpu_custom_call" | custom-call | tf_op jit(solution)/shard_map/pallas_call | solution.py:726
  151.3 1.9 %copy.15 = bf16[128,2048]{1,0:T(8,128)(2,1)} copy(bf16[128,2048]{1,0:T(8,128)(2,1)} %shard_map.127) | data formatting | bytes 1048576

commit v6 on v5

--- a/solution.py
+++ b/solution.py
@@ -45,7 +45,7 @@
     wg,
     wu,
     wd,
-    out,
+    out_hbm,
     w1,
     w2,
     w3,
@@ -71,6 +71,7 @@
     gains,
     lam_ref,
     base_ref,
+    out,
     local_sem,
     z_send,
     z_recv,
@@ -696,8 +697,18 @@
 
     last_one.arrive(0)
     lax.fori_loop(0, per, last, 0)
+    leave = [
+        pltpu.make_async_copy(
+            out.at[pl.ds(ch * chunk, chunk)], out_hbm.at[pl.ds(ch * chunk, chunk)], local_sem.at[ch]
+        )
+        for ch in (0, 1)
+    ]
+    leave[0].start()
     last_one.arrive(1)
     lax.fori_loop(per, 2 * per, last, 0)
+    leave[1].start()
+    leave[0].wait()
+    leave[1].wait()
     two[0][6]()
     two[1][6]()
     last_one.drain()
@@ -717,7 +728,6 @@
     heads = np.arange(2 * nx, dtype=np.float64)
     lam = -(4.0 / BLOCK) * (BLOCK / (32.0 * seq)) ** (heads / (H - 1))
     lam = jnp.asarray(np.repeat(lam[:, None], 128, axis=1).astype(np.float32))
-    vmem = pl.BlockSpec(memory_space=pltpu.VMEM)
     hbm = pl.BlockSpec(memory_space=pl.ANY)
     dma = pltpu.SemaphoreType.DMA
     far = nf // 2
@@ -727,7 +737,7 @@
         functools.partial(kernel, nf, nx),
         out_shape=jax.ShapeDtypeStruct((rows, width), BF16),
         in_specs=[hbm] * 13,
-        out_specs=vmem,
+        out_specs=hbm,
         scratch_shapes=[
             pltpu.VMEM((width, n1), BF16),
             pltpu.VMEM((wo.shape[0], width), BF16),
@@ -754,6 +764,7 @@
             pltpu.VMEM(gains.shape, F32),
             pltpu.VMEM(lam.shape, F32),
             pltpu.VMEM(base.shape, F32),
+            pltpu.VMEM((rows, width), BF16),
             dma((13,)),
             dma((24,)),
             dma((12, far)),

time: 153 us -> 153 us (level)
  no operation moved by 1% of the time
where the time goes in v6:
time: 153 us
  Pallas kernels  151 us (99%)
  local copies, waits for them, and re-layouts  1.88 us (1%)
    pallas_call x1, Pallas kernels, layer(): pl.pallas_call(functools.partial(kernel, nf, nx), out_shape=jax.ShapeDtyp...  151 us

profile of v6, /device:TPU:33, one launch (start us, length us, event | category | flops | bytes accessed | tf_op | source)
XLA Modules:
  0.0 153.1 jit_solution(9375780281441057201)
XLA Ops:
  0.0 151.2 %shard_map.127 = bf16[128,2048]{1,0:T(8,128)(2,1)} custom-call(bf16[128,2048]{1,0:T(8,128)(2,1)} %tok_hbm.1, f32[4,2048]{1,0:T(4,128)} %gains_hbm.1, f32[8,128]{1,0:T(8,128)} %constant.8.clone.lam_hbm, f32[2,256,128]{2,1,0:T(8,128)} %constant.6.clone.turn_hbm, f32[8,128]{1,0:T(8,128)} %constant.7.clone.base_hbm, bf16[128,256]{1,0:T(8,128)(2,1)} %wq.1, ...), custom_call_target="tpu_custom_call" | custom-call | tf_op jit(solution)/shard_map/pallas_call | solution.py:736
  151.2 1.9 %copy.15 = bf16[128,2048]{1,0:T(8,128)(2,1)} copy(bf16[128,2048]{1,0:T(8,128)(2,1)} %shard_map.127) | data formatting | bytes 1048576
